TPU v7x, 128 devices: a whole 4x4x4 slice. The times are simulated.
128 devices in a mesh: ep: 32 (over z, y, core), tp: 4 (over x).
Axes of the slice: x: 4, y: 4, z: 4, core: 2. Of those that a mesh axis runs over, the one named last changes fastest.
Arguments:
- tokens: bfloat16 [1536, 2048], P(('ep', 'tp')), may hold values from -6 to 6
- cache_latent: bfloat16 [1536, 1024, 512], P(('ep', 'tp')), may hold values from -1700 to 1700
- cache_rope: bfloat16 [1536, 64, 1024], P(('ep', 'tp')), may hold values from -6 to 6
- lengths: int32 [1536], P(('ep', 'tp')), may hold values from 128 to 1023, as said below
- attn_gain: bfloat16 [2048], replicated, may hold values from 0.099609375 to 1.8984375
- latent_gain: bfloat16 [512], replicated, may hold values from 0.099609375 to 1.8984375
- post_attn_gain: bfloat16 [2048], replicated, may hold values from 0.099609375 to 1.8984375
- ffn_gain: bfloat16 [2048], replicated, may hold values from 0.099609375 to 1.8984375
- post_ffn_gain: bfloat16 [2048], replicated, may hold values from 0.099609375 to 1.8984375
- w_query: bfloat16 [2048, 2048], P(None, 'tp'), may hold values from -0.125 to 0.125
- w_query_rot: bfloat16 [2048, 1024], P(None, 'tp'), may hold values from -0.125 to 0.125
- w_latent: bfloat16 [2048, 512], P(None, 'tp'), may hold values from -0.125 to 0.125
- w_key_rot: bfloat16 [2048, 64], replicated, may hold values from -0.125 to 0.125
- w_key_up: bfloat16 [512, 16, 128], P(None, 'tp'), may hold values from -0.25 to 0.25
- w_value_up: bfloat16 [512, 16, 128], P(None, 'tp'), may hold values from -0.25 to 0.25
- w_out: bfloat16 [2048, 2048], P('tp'), may hold values from -0.125 to 0.125
- route_logits: float32 [1536, 4], P('ep'), may hold values from -6 to 6
- routes: int32 [1536, 4], P('ep'), may hold values from 0 to 31, all different within a row; in each aligned block of 48 rows (0 to 47, 48 to 95, ...) at most 7 rows name the same one
- w_gate: bfloat16 [32, 2048, 2048], P('ep', None, 'tp'), may hold values from -0.3125 to 0.3125
- w_up: bfloat16 [32, 2048, 2048], P('ep', None, 'tp'), may hold values from -0.3125 to 0.3125
- w_down: bfloat16 [32, 2048, 2048], P('ep', 'tp'), may hold values from -0.125 to 0.125
Outputs:
- result: bfloat16 [1536, 2048], P(('ep', 'tp'))
- new_latent: bfloat16 [1536, 512], P(('ep', 'tp'))
- new_rope: bfloat16 [1536, 64], P(('ep', 'tp'))
Inputs may be any that keep to these rules, and one draw needn't show every extreme that they name: Each sequence's cache holds positions 0 to lengths - 1, and the new token stands at position lengths; some sequence has 1023 in every draw. `routes`: each row names 4 different experts; in each aligned block of 48 rows (the tokens of one index of ep) no expert is named more than 7 times, a bound that some block reaches.
All inputs are finite; a program needn't handle non-finite values.
Results may differ from a plain program's by a relative error of at most 0.019.
Values may be sent and summed in bfloat16 or wider, within the bound.
A program may use at most 128 MiB of HBM per device.

v0:
```python
import jax
import jax.numpy as jnp
from jax import lax
from jax.sharding import PartitionSpec as P

eps_norm = 1e-06
clamp_limit = 7.0
sigmoid_alpha = 1.702
theta_base = 10000.0


def from_everyone(array, axis):
    copies = jnp.broadcast_to(array, (lax.axis_size(axis), *array.shape))
    return lax.all_to_all(copies, axis, split_axis=0, concat_axis=0, tiled=True)


def laid_out(parts, dim):
    parts = jnp.moveaxis(parts, 0, dim)
    shape = parts.shape
    return parts.reshape(*shape[:dim], shape[dim] * shape[dim + 1], *shape[dim + 2 :])


def gather_directly(array, axis, dim):
    parts = from_everyone(array, axis)
    return laid_out(parts, dim)


def sent_together(arrays, axis, split_dim, concat_dim, along):
    both = jnp.concatenate(arrays, axis=along)
    result, at, outs = (
        lax.all_to_all(both, axis, split_axis=split_dim, concat_axis=concat_dim, tiled=True),
        0,
        [],
    )
    for a in arrays:
        outs.append(lax.slice_in_dim(result, at, at + a.shape[along], axis=along))
        at += a.shape[along]
    return tuple(outs)


def cut_along(array, dim, devices):
    before, after = (array.shape[:dim], array.shape[dim + 1 :])
    return jnp.moveaxis(array.reshape(*before, devices, -1, *after), dim, 0)


def sum_at_owner(array, axis, dim):
    parts = cut_along(array, dim, lax.axis_size(axis))
    arrived = lax.all_to_all(parts, axis, split_axis=0, concat_axis=0, tiled=True)
    return arrived.astype(jnp.float32).sum(axis=0)


def rms_scale(values, gain):
    mean_square = jnp.mean(values * values, axis=-1, keepdims=True)
    return values * lax.rsqrt(mean_square + eps_norm) * gain.astype(jnp.float32)


def rotate(values, positions):
    half = values.shape[-1] // 2
    freqs = theta_base ** (-jnp.arange(half, dtype=jnp.float32) / half)
    angles = positions[..., None] * freqs
    cosine = jnp.cos(angles)
    sine = jnp.sin(angles)
    first = values[..., :half]
    second = values[..., half:]
    return jnp.concatenate(
        [first * cosine - second * sine, second * cosine + first * sine], axis=-1
    )


def attend(
    query_latent, query_turned, cache_latent, cache_rope, new_latent, new_rope, lengths, scale
):
    sequences, heads, latent_size = query_latent.shape
    span = cache_latent.shape[1]
    stride = min(512, span)
    blocks_used = (jnp.max(lengths) + stride - 1) // stride

    def score_block(index, scores):
        offset = index * stride
        latents = lax.dynamic_slice_in_dim(cache_latent, offset, stride, 1)
        rotary = lax.dynamic_slice_in_dim(cache_rope, offset, stride, 2)
        block_scores = jnp.einsum(
            "shc,spc->shp", query_latent, latents, preferred_element_type=jnp.float32
        )
        block_scores = block_scores + jnp.einsum(
            "shr,srp->shp", query_turned, rotary, preferred_element_type=jnp.float32
        )
        return lax.dynamic_update_slice_in_dim(scores, block_scores * scale, offset, 2)

    scores = lax.fori_loop(
        0, blocks_used, score_block, jnp.zeros((sequences, heads, span), jnp.float32)
    )
    self_score = (
        jnp.einsum("shc,sc->sh", query_latent, new_latent, preferred_element_type=jnp.float32)
        + jnp.einsum("shr,sr->sh", query_turned, new_rope, preferred_element_type=jnp.float32)
    ) * scale
    valid = jnp.arange(span, dtype=jnp.int32)[None, None, :] < lengths[:, None, None]
    masked = jnp.where(valid, scores, -jnp.inf)
    highest = jnp.maximum(jnp.max(masked, axis=-1), self_score)
    raised = jnp.exp(masked - highest[..., None])
    raised_self = jnp.exp(self_score - highest)
    total = jnp.sum(raised, axis=-1) + raised_self
    probs = (raised / total[..., None]).astype(jnp.bfloat16)
    prob_self = (raised_self / total).astype(jnp.bfloat16)

    def read_block(index, summed):
        offset = index * stride
        latents = lax.dynamic_slice_in_dim(cache_latent, offset, stride, 1)
        weights = lax.dynamic_slice_in_dim(probs, offset, stride, 2)
        return summed + jnp.einsum(
            "shp,spc->shc", weights, latents, preferred_element_type=jnp.float32
        )

    summed = lax.fori_loop(
        0, blocks_used, read_block, jnp.zeros((sequences, heads, latent_size), jnp.float32)
    )
    summed = (
        summed
        + prob_self.astype(jnp.float32)[..., None] * new_latent.astype(jnp.float32)[:, None, :]
    )
    return summed.astype(jnp.bfloat16)


def body(
    tokens,
    cache_latent,
    cache_rope,
    lengths,
    attn_gain,
    latent_gain,
    post_attn_gain,
    ffn_gain,
    post_ffn_gain,
    w_query,
    w_query_rot,
    w_latent,
    w_key_rot,
    w_key_up,
    w_value_up,
    w_out,
    route_logits,
    routes,
    w_gate,
    w_up,
    w_down,
):
    own_rows, width = tokens.shape
    tensor_ways = lax.axis_size("tp")
    expert_ways = lax.axis_size("ep")
    latent_size, local_heads, key_size = w_key_up.shape
    rot_size = w_key_rot.shape[1]
    value_size = w_value_up.shape[2]
    group = own_rows * tensor_ways
    scale = (key_size + rot_size) ** (-0.5)
    token_values = tokens.astype(jnp.float32)
    normed = rms_scale(token_values, attn_gain).astype(jnp.bfloat16)
    key_raw = jnp.dot(normed, w_key_rot, preferred_element_type=jnp.float32).astype(jnp.bfloat16)
    group_rows = gather_directly(normed, "tp", 0)
    stacked = jnp.concatenate([w_query, w_query_rot, w_latent], axis=1)
    projected = jnp.dot(group_rows, stacked, preferred_element_type=jnp.float32).astype(
        jnp.bfloat16
    )
    plain_cols = local_heads * key_size
    rotary_cols = local_heads * rot_size
    query_plain = projected[:, :plain_cols].reshape(group, local_heads, key_size)
    query_rotary = projected[:, plain_cols : plain_cols + rotary_cols].reshape(
        group, local_heads, rot_size
    )
    latent_part = projected[:, plain_cols + rotary_cols :]
    query_latent = jnp.einsum(
        "ghn,chn->ghc", query_plain, w_key_up, preferred_element_type=jnp.float32
    ).astype(jnp.bfloat16)
    query_latent, query_rotary, latent_raw = (
        *sent_together((query_latent, query_rotary), "tp", 0, 1, 2),
        lax.all_to_all(latent_part, "tp", split_axis=0, concat_axis=1, tiled=True),
    )
    positions = lengths.astype(jnp.float32)
    new_latent = rms_scale(latent_raw.astype(jnp.float32), latent_gain).astype(jnp.bfloat16)
    new_rope = rotate(key_raw.astype(jnp.float32), positions).astype(jnp.bfloat16)
    query_turned = rotate(query_rotary.astype(jnp.float32), positions[:, None]).astype(jnp.bfloat16)
    head_latent = attend(
        query_latent, query_turned, cache_latent, cache_rope, new_latent, new_rope, lengths, scale
    )
    head_latent = lax.all_to_all(head_latent, "tp", split_axis=1, concat_axis=0, tiled=True)
    values = jnp.einsum("ghc,chv->ghv", head_latent, w_value_up, preferred_element_type=jnp.float32)
    values = values.astype(jnp.bfloat16).reshape(group, local_heads * value_size)
    attn = sum_at_owner(
        jnp.dot(values, w_out, preferred_element_type=jnp.float32).astype(jnp.bfloat16), "tp", 0
    ).astype(jnp.bfloat16)
    mixed = (token_values + rms_scale(attn.astype(jnp.float32), post_attn_gain)).astype(
        jnp.bfloat16
    )
    ffn_input = rms_scale(mixed.astype(jnp.float32), ffn_gain).astype(jnp.bfloat16)
    group_inputs = gather_directly(ffn_input, "tp", 0)
    top_k = routes.shape[1]
    capacity = (group * top_k + expert_ways - 1) // expert_ways + 1
    flat_routes = routes.reshape(-1)
    onehot = (flat_routes[:, None] == jnp.arange(expert_ways, dtype=jnp.int32)[None, :]).astype(
        jnp.int32
    )
    rank = jnp.sum((jnp.cumsum(onehot, axis=0) - onehot) * onehot, axis=1)
    slot_of = (flat_routes * capacity + rank).reshape(group, top_k)
    slot_ids = jnp.arange(expert_ways * capacity, dtype=jnp.int32)
    hits = slot_of[:, :, None] == slot_ids[None, None, :]
    dispatch_map = jnp.any(hits, axis=1).astype(jnp.bfloat16)
    slots = jnp.einsum("gs,gd->sd", dispatch_map, group_inputs, preferred_element_type=jnp.float32)
    slots = slots.astype(jnp.bfloat16).reshape(expert_ways, capacity, width)
    gate_local = w_gate[0]
    up_local = w_up[0]
    down_local = w_down[0]
    received = lax.all_to_all(slots, "ep", split_axis=0, concat_axis=0, tiled=True)
    sources, count, _ = received.shape
    flat = received.reshape(sources * count, width)
    gate = jnp.minimum(jnp.dot(flat, gate_local, preferred_element_type=jnp.float32), clamp_limit)
    upward = jnp.clip(
        jnp.dot(flat, up_local, preferred_element_type=jnp.float32), -clamp_limit, clamp_limit
    )
    active = ((upward + 1.0) * gate * jax.nn.sigmoid(sigmoid_alpha * gate)).astype(jnp.bfloat16)
    partial_out = jnp.dot(active, down_local, preferred_element_type=jnp.float32)
    partial_out = partial_out.reshape(sources, count, width)
    summed = sum_at_owner(partial_out.astype(jnp.bfloat16), "tp", 2).astype(jnp.bfloat16)
    returned = lax.all_to_all(summed, "ep", split_axis=0, concat_axis=0, tiled=True)
    route_weights = jax.nn.softmax(route_logits, axis=-1)
    combine = jnp.sum(jnp.where(hits, route_weights[:, :, None], 0.0), axis=1)
    moe_part = jnp.dot(
        combine,
        returned.reshape(-1, returned.shape[2]).astype(jnp.float32),
        precision=lax.Precision.HIGHEST,
    ).astype(jnp.bfloat16)
    moe = lax.all_to_all(moe_part, "tp", split_axis=0, concat_axis=1, tiled=True)
    result = (mixed.astype(jnp.float32) + rms_scale(moe.astype(jnp.float32), post_ffn_gain)).astype(
        jnp.bfloat16
    )
    return (result, new_latent, new_rope)


def solution(mesh):
    return jax.shard_map(
        body,
        mesh=mesh,
        in_specs=(
            P(("ep", "tp"), None),
            P(("ep", "tp"), None, None),
            P(("ep", "tp"), None, None),
            P(("ep", "tp")),
            P(),
            P(),
            P(),
            P(),
            P(),
            P(None, "tp"),
            P(None, "tp"),
            P(None, "tp"),
            P(),
            P(None, "tp", None),
            P(None, "tp", None),
            P("tp", None),
            P("ep", None),
            P("ep", None),
            P("ep", None, "tp"),
            P("ep", None, "tp"),
            P("ep", "tp", None),
        ),
        out_specs=(P(("ep", "tp"), None), P(("ep", "tp"), None), P(("ep", "tp"), None)),
        check_vma=False,
    )
```

profile of v0, /device:TPU:1, one launch (start us, length us, event | category | flops | bytes accessed | tf_op | source)
XLA Modules:
  0.0 171.0 jit_solution(12454278551004720385)
XLA Ops:
  0.6 0.8 convert_element_type.148
  1.5 1.0 fusion.60
  2.5 0.9 fusion.62
  3.4 0.7 broadcast_in_dim.31
  4.1 4.8 %all-to-all-start = ((bf16[4,12,2048]{2,1,0:T(8,128)(2,1)}), bf16[4,12,2048]{2,1,0:T(8,128)(2,1)S(1)}, u32[]{:S(2)}, u32[]{:S(2)}) async-start(bf16[4,12,2048]{2,1,0:T(8,128)(2,1)} %broadcast_in_dim.31), calls=%async_computation | async-start | bytes 524288 | tf_op jit(solution)/shard_map/all_to_all | solution.py:14
  8.9 1.4 fusion.89
  10.3 0.7 iota_compare_fusion.1
  11.1 1.1 fusion.49
  12.2 0.8 copy.150
  13.9 0.7 convert_element_type.159
  14.7 2.8 %fusion.45 = bf16[48,896]{1,0:T(8,128)(2,1)S(1)} fusion(bf16[48,2048]{1,0:T(8,128)(2,1)S(1)} %reshape.235, bf16[2048,128]{1,0:T(8,128)(2,1)} %param.36, bf16[2048,256]{1,0:T(8,128)(2,1)} %param.35, bf16[2048,512]{1,0:T(8,128)(2,1)} %param.34), kind=kOutput, calls=%fused_computation.36 | convolution fusion | flops 187213824 | bytes 3952640 | tf_op jit(solution)/shard_map/dot_general | solution.py:160
  17.5 0.3 fusion.44
  18.0 0.6 all_to_all.69
  18.6 4.2 %all-to-all-start.2 = ((bf16[4,12,128]{2,1,0:T(8,128)(2,1)}), bf16[4,12,128]{2,1,0:T(8,128)(2,1)S(1)}, u32[]{:S(2)}, u32[]{:S(2)}) async-start(bf16[4,12,128]{2,1,0:T(8,128)(2,1)} %all_to_all.69), calls=%async_computation.2 | async-start | bytes 32768 | tf_op jit(solution)/shard_map/all_to_all | solution.py:175
  22.8 0.8 copy.141
  23.6 3.4 %all-to-all-done.2 = bf16[4,12,128]{2,1,0:T(8,128)(2,1)S(1)} async-done(((bf16[4,12,128]{2,1,0:T(8,128)(2,1)}), bf16[4,12,128]{2,1,0:T(8,128)(2,1)S(1)}, u32[]{:S(2)}, u32[]{:S(2)}) %all-to-all-start.2) | async-done | bytes 12320 | tf_op jit(solution)/shard_map/all_to_all | solution.py:175
  27.0 3.4 %all-to-all-start.1 = ((bf16[48,4,576]{2,1,0:T(4,128)(2,1)}), bf16[48,4,576]{2,1,0:T(4,128)(2,1)S(1)}, u32[]{:S(2)}, u32[]{:S(2)}) async-start(bf16[48,4,576]{2,1,0:T(4,128)(2,1)} %copy.141), calls=%async_computation.1 | async-start | bytes 491520 | tf_op jit(solution)/shard_map/all_to_all | solution.py:31
  30.7 5.1 %all-to-all-done.1 = bf16[48,4,576]{2,1,0:T(4,128)(2,1)S(1)} async-done(((bf16[48,4,576]{2,1,0:T(4,128)(2,1)}), bf16[48,4,576]{2,1,0:T(4,128)(2,1)S(1)}, u32[]{:S(2)}, u32[]{:S(2)}) %all-to-all-start.1) | async-done | bytes 221216 | tf_op jit(solution)/shard_map/all_to_all | solution.py:31
  36.4 4.9 %while.20 = (s32[]{:T(128)}, f32[12,16,1024]{2,1,0:T(8,128)S(1)}, s32[]{:T(128)}, bf16[12,1024,512]{2,1,0:T(8,128)(2,1)}, bf16[12,16,512]{2,1,0:T(8,128)(2,1)S(1...) while((s32[]{:T(128)}, f32[12,16,1024]{2,1,0:T(8,128)S(1)}, ...), condition=%wide.region_3.4_spmd, body=%wide.region_2.0_spmd.sunk | while | flops 113442824 | bytes 14795963 | solution.py:90
  36.4 4.6 %fusion.117 = f32[12,512,16]{1,2,0:T(8,128)S(1)} fusion(bf16[12,16,512]{2,1,0:T(8,128)(2,1)S(1)} %get-tuple-element.211, bf16[12,1024,512]{2,1,0:T(8,128)(2,1)} %get-tuple-element.210, s32[]{:T(128)S(6)} %select_n.34), kind=kOutput, calls=%fused_computation.clone.1 | convolution fusion | flops 100663296 | bytes 6881284 | tf_op jit(solution)/shard_map/while/body/shc,spc->shp/dot_general | solution.py:82
  41.1 0.2 fusion.118
  41.5 0.2 fusion.75
  41.6 0.2 select_reduce_fusion
  41.8 0.3 fusion.50
  42.1 0.3 divide_convert_fusion
  42.4 3.7 %while.21 = (s32[]{:T(128)}, f32[12,16,512]{2,1,0:T(8,128)S(1)}, s32[]{:T(128)}, bf16[12,16,1024]{2,1,0:T(8,128)(2,1)S(1)}, bf16[12,1024,512]{2,1,0:T(8,128)(2,1...) while((s32[]{:T(128)}, f32[12,16,512]{2,1,0:T(8,128)S(1)}, s32[]{:T(128)}, ...), condition=%wide.region_8.9_spmd, body=%wide.region_7.8_spmd.sunk | while | flops 100761608 | bytes 7275659 | solution.py:114
  42.5 3.7 %fusion.121 = f32[12,16,512]{2,1,0:T(8,128)S(1)} fusion(f32[12,16,512]{2,1,0:T(8,128)S(1)} %get-tuple-element.228, bf16[12,1024,512]{2,1,0:T(8,128)(2,1)} %get-tuple-element.240, s32[]{:T(128)S(6)} %select_n.35, bf16[12,16,1024]{2,1,0:T(8,128)(2,1)S(1)} %get-tuple-element.239), kind=kOutput, calls=%fused_computation.11.clone.1 | convolution fusion | flops 100761600 | bytes 7275520 | tf_op jit(solution)/shard_map/while/body/shp,spc->shc/dot_general | solution.py:110
  46.3 0.9 fusion.52
  47.2 10.8 %all-to-all-start.3 = ((bf16[12,16,512]{2,0,1:T(8,128)(2,1)}), bf16[12,16,512]{2,0,1:T(8,128)(2,1)S(1)}, u32[]{:S(2)}, u32[]{:S(2)}) async-start(bf16[12,16,512]{2,0,1:T(8,128)(2,1)} %fusion.52), calls=%async_computation.3 | async-start | bytes 524288 | tf_op jit(solution)/shard_map/all_to_all | solution.py:184
  58.0 0.6 reduce-window.6
  58.6 0.2 slice_reduce_fusion
  58.8 4.7 %all-to-all-done.3 = bf16[12,16,512]{2,0,1:T(8,128)(2,1)S(1)} async-done(((bf16[12,16,512]{2,0,1:T(8,128)(2,1)}), bf16[12,16,512]{2,0,1:T(8,128)(2,1)S(1)}, u32[]{:S(2)}, u32[]{:S(2)}) %all-to-all-start.3) | async-done | bytes 196640 | tf_op jit(solution)/shard_map/all_to_all | solution.py:184
  63.5 0.2 copy.146
  63.7 1.3 fusion.48
  65.0 2.1 %convolution_convert_fusion.2 = bf16[48,2048]{1,0:T(8,128)(2,1)S(1)} fusion(bf16[512,2048]{1,0:T(8,128)(2,1)} %param.40, bf16[4,6,8,128]{3,2,1,0:T(8,128)(2,1)S(1)} %fusion.48), kind=kOutput, calls=%fused_computation.22 | convolution fusion | flops 100761600 | bytes 2342912 | tf_op jit(solution)/shard_map/dot_general | solution.py:188
  67.1 0.7 reshape.239
  67.9 3.4 %all-to-all-start.4 = ((bf16[4,12,2048]{2,1,0:T(8,128)(2,1)}), bf16[4,12,2048]{2,1,0:T(8,128)(2,1)S(1)}, u32[]{:S(2)}, u32[]{:S(2)}) async-start(bf16[4,12,2048]{2,1,0:T(8,128)(2,1)} %reshape.239), calls=%async_computation.4 | async-start | bytes 524288 | tf_op jit(solution)/shard_map/all_to_all | solution.py:48
  71.6 5.2 %all-to-all-done.4 = bf16[4,12,2048]{2,1,0:T(8,128)(2,1)S(1)} async-done(((bf16[4,12,2048]{2,1,0:T(8,128)(2,1)}), bf16[4,12,2048]{2,1,0:T(8,128)(2,1)S(1)}, u32[]{:S(2)}, u32[]{:S(2)}) %all-to-all-start.4) | async-done | bytes 196640 | tf_op jit(solution)/shard_map/all_to_all | solution.py:48
  76.8 0.1 fusion.57
  77.0 0.2 fusion.64
  77.3 0.7 broadcast_in_dim.35
  78.0 3.4 %all-to-all-start.5 = ((bf16[4,12,2048]{2,1,0:T(8,128)(2,1)}), bf16[4,12,2048]{2,1,0:T(8,128)(2,1)S(1)}, u32[]{:S(2)}, u32[]{:S(2)}) async-start(bf16[4,12,2048]{2,1,0:T(8,128)(2,1)} %broadcast_in_dim.35), calls=%async_computation.5 | async-start | bytes 524288 | tf_op jit(solution)/shard_map/all_to_all | solution.py:14
  81.5 5.4 %all-to-all-done.5 = bf16[4,12,2048]{2,1,0:T(8,128)(2,1)S(1)} async-done(((bf16[4,12,2048]{2,1,0:T(8,128)(2,1)}), bf16[4,12,2048]{2,1,0:T(8,128)(2,1)S(1)}, u32[]{:S(2)}, u32[]{:S(2)}) %all-to-all-start.5) | async-done | bytes 196640 | tf_op jit(solution)/shard_map/all_to_all | solution.py:14
  87.0 1.4 convolution_convert_fusion.1
  88.3 1.5 reshape.243
  89.8 33.4 %all_to_all.92 = bf16[32,7,2048]{2,1,0:T(8,128)(2,1)} all-to-all(bf16[32,7,2048]{2,1,0:T(8,128)(2,1)S(1)} %reshape.243), channel_id=1, replica_groups=mesh['ep'=32,'tp'=4] {'ep'}, dimensions={0} | all-to-all | bytes 1835008 | tf_op jit(solution)/shard_map/all_to_all | solution.py:211
  123.2 1.5 reshape.244
  124.7 2.4 %fusion.32 = f32[224,512]{1,0:T(8,128)S(1)} fusion(bf16[224,2048]{1,0:T(8,128)(2,1)S(1)} %reshape.244, bf16[1,2048,512]{2,1,0:T(8,128)(2,1)} %param.43), kind=kOutput, calls=%fused_computation.30 | convolution fusion | flops 469876736 | bytes 3473408 | tf_op jit(solution)/shard_map/dot_general | solution.py:214
  127.1 0.7 fusion.41
  127.9 0.7 convolution_convert_fusion
  128.5 1.0 copy.227
  129.6 3.5 %all-to-all-start.7 = ((bf16[4,32,7,512]{3,1,2,0:T(8,128)(2,1)}), bf16[4,32,7,512]{3,1,2,0:T(8,128)(2,1)S(1)}, u32[]{:S(2)}, u32[]{:S(2)}) async-start(bf16[4,32,7,512]{3,1,2,0:T(8,128)(2,1)} %bitcast.126), calls=%async_computation.7 | async-start | bytes 1835008 | tf_op jit(solution)/shard_map/all_to_all | solution.py:48
  133.2 13.3 %all-to-all-done.7 = bf16[4,32,7,512]{3,1,2,0:T(8,128)(2,1)S(1)} async-done(((bf16[4,32,7,512]{3,1,2,0:T(8,128)(2,1)}), bf16[4,32,7,512]{3,1,2,0:T(8,128)(2,1)S(1)}, u32[]{:S(2)}, u32[]{:S(2)}) %all-to-all-start.7) | async-done | bytes 917536 | tf_op jit(solution)/shard_map/all_to_all | solution.py:48
  146.5 0.2 reduce_sum.117
  146.6 0.8 copy.157
  147.4 4.8 %all-to-all-start.8 = ((bf16[32,7,512]{2,1,0:T(8,128)(2,1)}), bf16[32,7,512]{2,1,0:T(8,128)(2,1)S(1)}, u32[]{:S(2)}, u32[]{:S(2)}) async-start(bf16[32,7,512]{2,1,0:T(8,128)(2,1)} %copy.157), calls=%async_computation.8 | async-start | bytes 524288 | tf_op jit(solution)/shard_map/all_to_all | solution.py:222
  152.4 8.8 %all-to-all-done.8 = bf16[32,7,512]{2,1,0:T(8,128)(2,1)S(1)} async-done(((bf16[32,7,512]{2,1,0:T(8,128)(2,1)}), bf16[32,7,512]{2,1,0:T(8,128)(2,1)S(1)}, u32[]{:S(2)}, u32[]{:S(2)}) %all-to-all-start.8) | async-done | bytes 229408 | tf_op jit(solution)/shard_map/all_to_all | solution.py:222
  161.3 0.2 convolution_convert_fusion.4
  161.5 0.6 all_to_all.80
  162.2 3.3 %all-to-all-start.9 = ((bf16[4,12,512]{2,1,0:T(8,128)(2,1)}), bf16[4,12,512]{2,1,0:T(8,128)(2,1)S(1)}, u32[]{:S(2)}, u32[]{:S(2)}) async-start(bf16[4,12,512]{2,1,0:T(8,128)(2,1)} %all_to_all.80), calls=%async_computation.9 | async-start | bytes 131072 | tf_op jit(solution)/shard_map/all_to_all | solution.py:230
  165.5 0.7 pad_maximum_fusion.2
  166.2 3.8 %all-to-all-done.9 = bf16[4,12,512]{2,1,0:T(8,128)(2,1)S(1)} async-done(((bf16[4,12,512]{2,1,0:T(8,128)(2,1)}), bf16[4,12,512]{2,1,0:T(8,128)(2,1)S(1)}, u32[]{:S(2)}, u32[]{:S(2)}) %all-to-all-start.9) | async-done | bytes 49184 | tf_op jit(solution)/shard_map/all_to_all | solution.py:230
  170.1 0.1 fusion.59
  170.2 0.7 fusion.67
  (82 shorter events, 2.7 us)
Async XLA Ops:
  0.6 127.2 %copy-start = (bf16[1,512,2048]{2,1,0:T(8,128)(2,1)S(1)}, bf16[1,512,2048]{2,1,0:T(8,128)(2,1)}, u32[]{:S(2)}) copy-start(bf16[1,512,2048]{2,1,0:T(8,128)(2,1)} %param.45) | copy-start | bytes 6291460
  4.1 10.5 %all-to-all-start = ((bf16[4,12,2048]{2,1,0:T(8,128)(2,1)}), bf16[4,12,2048]{2,1,0:T(8,128)(2,1)S(1)}, u32[]{:S(2)}, u32[]{:S(2)}) async-start(bf16[4,12,2048]{2,1,0:T(8,128)(2,1)} %broadcast_in_dim.31), calls=%async_computation | async-start | bytes 524288 | tf_op jit(solution)/shard_map/all_to_all | solution.py:14
  14.7 2.9 %copy-start.3 = (bf16[512,4,128]{2,1,0:T(4,128)(2,1)S(1)}, bf16[512,4,128]{2,1,0:T(4,128)(2,1)}, u32[]{:S(2)}) copy-start(bf16[512,4,128]{2,1,0:T(4,128)(2,1)} %param.38) | copy-start | bytes 1572868
  18.6 8.4 %all-to-all-start.2 = ((bf16[4,12,128]{2,1,0:T(8,128)(2,1)}), bf16[4,12,128]{2,1,0:T(8,128)(2,1)S(1)}, u32[]{:S(2)}, u32[]{:S(2)}) async-start(bf16[4,12,128]{2,1,0:T(8,128)(2,1)} %all_to_all.69), calls=%async_computation.2 | async-start | bytes 32768 | tf_op jit(solution)/shard_map/all_to_all | solution.py:175
  27.0 8.8 %all-to-all-start.1 = ((bf16[48,4,576]{2,1,0:T(4,128)(2,1)}), bf16[48,4,576]{2,1,0:T(4,128)(2,1)S(1)}, u32[]{:S(2)}, u32[]{:S(2)}) async-start(bf16[48,4,576]{2,1,0:T(4,128)(2,1)} %copy.141), calls=%async_computation.1 | async-start | bytes 491520 | tf_op jit(solution)/shard_map/all_to_all | solution.py:31
  30.7 10.8 %copy-start.5 = (bf16[12,512]{1,0:T(8,128)(2,1)}, bf16[12,512]{1,0:T(8,128)(2,1)S(1)}, u32[]{:S(2)}) copy-start(bf16[12,512]{1,0:T(8,128)(2,1)S(1)} %get-tuple-element.98) | copy-start | bytes 36868
  36.4 4.7 %copy-start.1 = (bf16[12,64,1024]{2,1,0:T(8,128)(2,1)S(1)}, bf16[12,64,1024]{2,1,0:T(8,128)(2,1)}, u32[]{:S(2)}) copy-start(bf16[12,64,1024]{2,1,0:T(8,128)(2,1)} %get-tuple-element.212) | copy-start | bytes 4718596 | tf_op jit(solution)/shard_map/while
  47.2 16.3 %all-to-all-start.3 = ((bf16[12,16,512]{2,0,1:T(8,128)(2,1)}), bf16[12,16,512]{2,0,1:T(8,128)(2,1)S(1)}, u32[]{:S(2)}, u32[]{:S(2)}) async-start(bf16[12,16,512]{2,0,1:T(8,128)(2,1)} %fusion.52), calls=%async_computation.3 | async-start | bytes 524288 | tf_op jit(solution)/shard_map/all_to_all | solution.py:184
  63.7 7.7 %copy-start.7 = (bf16[2048]{0:T(1024)(128)(2,1)S(1)}, bf16[2048]{0:T(1024)(128)(2,1)}, u32[]{:S(2)}) copy-start(bf16[2048]{0:T(1024)(128)(2,1)} %param.31) | copy-start | bytes 12292
  63.7 7.7 %copy-start.8 = (bf16[2048]{0:T(1024)(128)(2,1)S(1)}, bf16[2048]{0:T(1024)(128)(2,1)}, u32[]{:S(2)}) copy-start(bf16[2048]{0:T(1024)(128)(2,1)} %param.32) | copy-start | bytes 12292
  65.0 12.0 %copy-start.2 = (bf16[12,2048]{1,0:T(8,128)(2,1)S(1)}, bf16[12,2048]{1,0:T(8,128)(2,1)}, u32[]{:S(2)}) copy-start(bf16[12,2048]{1,0:T(8,128)(2,1)} %param.25) | copy-start | bytes 147460
  65.0 16.4 %copy-start.6 = (s32[48,4]{0,1:T(4,128)S(1)}, s32[48,4]{0,1:T(4,128)}, u32[]{:S(2)}) copy-start(s32[48,4]{0,1:T(4,128)} %param.42) | copy-start | bytes 2308
  67.9 8.9 %all-to-all-start.4 = ((bf16[4,12,2048]{2,1,0:T(8,128)(2,1)}), bf16[4,12,2048]{2,1,0:T(8,128)(2,1)S(1)}, u32[]{:S(2)}, u32[]{:S(2)}) async-start(bf16[4,12,2048]{2,1,0:T(8,128)(2,1)} %reshape.239), calls=%async_computation.4 | async-start | bytes 524288 | tf_op jit(solution)/shard_map/all_to_all | solution.py:48
  78.0 8.9 %all-to-all-start.5 = ((bf16[4,12,2048]{2,1,0:T(8,128)(2,1)}), bf16[4,12,2048]{2,1,0:T(8,128)(2,1)S(1)}, u32[]{:S(2)}, u32[]{:S(2)}) async-start(bf16[4,12,2048]{2,1,0:T(8,128)(2,1)} %broadcast_in_dim.35), calls=%async_computation.5 | async-start | bytes 524288 | tf_op jit(solution)/shard_map/all_to_all | solution.py:14
  124.7 2.4 %copy-start.10 = (bf16[1,2048,512]{2,1,0:T(8,128)(2,1)S(1)}, bf16[1,2048,512]{2,1,0:T(8,128)(2,1)}, u32[]{:S(2)}) copy-start(bf16[1,2048,512]{2,1,0:T(8,128)(2,1)} %param.44) | copy-start | bytes 6291460
  128.5 4.6 %copy-start.4 = (f32[48,4]{0,1:T(4,128)S(1)}, f32[48,4]{0,1:T(4,128)}, u32[]{:S(2)}) copy-start(f32[48,4]{0,1:T(4,128)} %param.41) | copy-start | bytes 2308
  129.6 16.9 %all-to-all-start.7 = ((bf16[4,32,7,512]{3,1,2,0:T(8,128)(2,1)}), bf16[4,32,7,512]{3,1,2,0:T(8,128)(2,1)S(1)}, u32[]{:S(2)}, u32[]{:S(2)}) async-start(bf16[4,32,7,512]{3,1,2,0:T(8,128)(2,1)} %bitcast.126), calls=%async_computation.7 | async-start | bytes 1835008 | tf_op jit(solution)/shard_map/all_to_all | solution.py:48
  133.1 33.0 %copy-start.9 = (bf16[2048]{0:T(1024)(128)(2,1)S(1)}, bf16[2048]{0:T(1024)(128)(2,1)}, u32[]{:S(2)}) copy-start(bf16[2048]{0:T(1024)(128)(2,1)} %param.33) | copy-start | bytes 12292
  147.4 13.8 %all-to-all-start.8 = ((bf16[32,7,512]{2,1,0:T(8,128)(2,1)}), bf16[32,7,512]{2,1,0:T(8,128)(2,1)S(1)}, u32[]{:S(2)}, u32[]{:S(2)}) async-start(bf16[32,7,512]{2,1,0:T(8,128)(2,1)} %copy.157), calls=%async_computation.8 | async-start | bytes 524288 | tf_op jit(solution)/shard_map/all_to_all | solution.py:222
  162.2 7.7 %all-to-all-start.9 = ((bf16[4,12,512]{2,1,0:T(8,128)(2,1)}), bf16[4,12,512]{2,1,0:T(8,128)(2,1)S(1)}, u32[]{:S(2)}, u32[]{:S(2)}) async-start(bf16[4,12,512]{2,1,0:T(8,128)(2,1)} %all_to_all.80), calls=%async_computation.9 | async-start | bytes 131072 | tf_op jit(solution)/shard_map/all_to_all | solution.py:230
where the time goes:
time: 172 us; the launch traced here: 171 us
  waiting for transfers between devices  49.6 us (29%)
  starting transfers between devices  41.7 us (24%)
  blocking collectives  33.4 us (19%)
  matrix products  21.8 us (13%)
  local copies, waits for them, and re-layouts  11.4 us (7%)
  other arithmetic  11.1 us (6%)
  between operations  1.85 us (1%)
    all_to_all x1, blocking collectives, body(): lax.all_to_all(slots, 'ep', split_axis=0, concat_axis=0, tiled=True)  33.4 us
    all_to_all x2, waiting for transfers between devices, sum_at_owner(): lax.all_to_all(parts, axis, split_axis=0, concat_axis=0, tiled=True)  18.5 us
    all_to_all x1, starting transfers between devices, body(): lax.all_to_all(head_latent, 'tp', split_axis=1, concat_axis=0, tiled=True)  10.8 us
    all_to_all x1, waiting for transfers between devices, body(): lax.all_to_all(summed, 'ep', split_axis=0, concat_axis=0, tiled=True)  8.8 us
    all_to_all x2, starting transfers between devices, from_everyone(): return lax.all_to_all(copies, axis, split_axis=0, concat_axis=0, tiled=True)  8.23 us
    all_to_all x2, starting transfers between devices, sum_at_owner(): lax.all_to_all(parts, axis, split_axis=0, concat_axis=0, tiled=True)  6.91 us
    all_to_all x2, waiting for transfers between devices, from_everyone(): return lax.all_to_all(copies, axis, split_axis=0, concat_axis=0, tiled=True)  5.37 us
    all_to_all x1, waiting for transfers between devices, sent_together(): lax.all_to_all(both, axis, split_axis=split_dim, concat_axis=concat_dim,...  5.14 us
  transfers between devices with their start and end apart: 9, of which 8 were waited for; matrix products, arithmetic and copies ran while one was open for 5% of the time, Pallas kernels for 0%

commit v1 on v0

v1 whole, which is shorter than its diff:
```python
import functools
import math

import jax
import jax.numpy as jnp
from jax import lax
from jax.experimental import pallas as pl
from jax.experimental.pallas import tpu as pltpu
from jax.sharding import PartitionSpec as P

MESH = pl.DeviceIdType.MESH
eps_norm = 1e-06
clamp_limit = 7.0
sigmoid_alpha = 1.702
theta_base = 10000.0
f32 = jnp.float32
bf16 = jnp.bfloat16

SEQ = 12
PAD = 16
D = 2048
LAT = 512
ROT = 64
LEN = 1024
HL = 4
TP = 4
EP = 32
CAPP = 8
MSG = HL * LAT + HL * ROT + 128


def hops(a):
    return min(a, 4 - a)


far_first = sorted(range(1, EP), key=lambda d: -(hops(d // 8) + hops((d // 2) % 4)))


def ep_shift(me, d, sign):
    z, y, c = me // 8, (me // 2) % 4, me % 2
    dz, dy, dc = d // 8, (d // 2) % 4, d % 2
    if sign < 0:
        dz, dy = (4 - dz) % 4, (4 - dy) % 4
    return ((z + dz) % 4) * 8 + ((y + dy) % 4) * 2 + (c + dc) % 2


def mm(a, b):
    return lax.dot_general(a, b, (((1,), (0,)), ((), ())), preferred_element_type=f32)


def mm_nt(a, b):
    return lax.dot_general(a, b, (((1,), (1,)), ((), ())), preferred_element_type=f32)


def rms(v, gain):
    mean_square = jnp.mean(v * v, axis=-1, keepdims=True)
    return v * lax.rsqrt(mean_square + eps_norm) * gain


def layer_kernel(
    lens,
    tok_in,
    routes_in,
    logits_in,
    g_attn,
    g_lat,
    g_post,
    g_ffn,
    g_post2,
    h_clat,
    h_crope,
    h_wq,
    h_wqr,
    h_wl,
    h_wkr,
    h_wku,
    h_wvu,
    h_wo,
    h_wg,
    h_wu,
    h_wd,
    out_ref,
    lat_ref,
    rope_ref,
    tok32,
    nbuf,
    wq,
    wqr,
    wl,
    wkr,
    wku,
    wvu,
    wtmp,
    wkh,
    wvh,
    msg_s,
    msg_r,
    cache,
    rope,
    A,
    A2,
    Q,
    Qr,
    S,
    Pb,
    ps_ref,
    O,
    hl_s,
    hl_r,
    wo,
    p_s,
    p_r,
    gbuf,
    mixed_ref,
    r64,
    l64,
    Dm,
    Cm,
    X,
    R,
    Y,
    T,
    wg,
    wu,
    wd,
    m_s,
    m_r,
    lsem,
    csem,
    rsem,
    tss,
    trs,
    dss,
    drs,
    ess,
    ers,
):
    me = lax.axis_index("ep")
    t = lax.axis_index("tp")
    barrier = pltpu.get_barrier_semaphore()
    for d in (1, 2, 3):
        pl.semaphore_signal(barrier, inc=1, device_id={"tp": (t + d) % TP}, device_id_type=MESH)
    for d in far_first:
        pl.semaphore_signal(barrier, inc=1, device_id={"ep": ep_shift(me, d, 1)}, device_id_type=MESH)

    def local(src, dst, i):
        return pltpu.make_async_copy(src, dst, lsem.at[i])

    c_wq = local(h_wq, wq, 0)
    c_wqr = local(h_wqr, wqr, 1)
    c_wl = local(h_wl, wl, 2)
    c_wkr = local(h_wkr, wkr, 3)
    c_wku = local(h_wku, wku, 4)
    c_wvu = local(h_wvu, wvu, 5)
    c_wo = local(h_wo, wo, 6)
    c_wg = local(h_wg.at[0], wg, 7)
    c_wu = local(h_wu.at[0], wu, 8)
    c_wd = local(h_wd.at[0], wd, 9)
    for c in (c_wku, c_wvu, c_wq, c_wqr, c_wl, c_wkr):
        c.start()

    def cache_copy(s):
        return pltpu.make_async_copy(h_clat.at[s], cache.at[s], csem.at[s])

    c_rope = pltpu.make_async_copy(h_crope, rope, rsem)

    def tp_copies(phase, src, dst):
        out = []
        for d in (2, 1, 3):
            j = (t + d) % TP
            out.append(
                pltpu.make_async_remote_copy(
                    src_ref=src(j),
                    dst_ref=dst,
                    send_sem=tss.at[phase, d],
                    recv_sem=trs.at[phase, d],
                    device_id={"tp": j},
                    device_id_type=MESH,
                )
            )
        return out

    tok32[...] = jnp.zeros((PAD, D), f32)
    tok32[0:SEQ, :] = tok_in[...].astype(f32)
    normed = rms(tok32[...], g_attn[...].astype(f32)).astype(bf16)
    nbuf[t] = normed
    pl.semaphore_wait(barrier, 34)
    ph0 = tp_copies(0, lambda j: nbuf.at[t], nbuf.at[t])
    for c in ph0:
        c.start()
    c_rope.start()
    for s in range(SEQ):
        cache_copy(s).start()
    for c in (c_wo, c_wg, c_wu, c_wd):
        c.start()

    r64[...] = jnp.full((TP * PAD, 4), -1, jnp.int32)
    l64[...] = jnp.zeros((TP * PAD, 4), f32)
    for j in range(TP):
        r64[PAD * j : PAD * j + SEQ, :] = routes_in[SEQ * j : SEQ * (j + 1), :]
        l64[PAD * j : PAD * j + SEQ, :] = logits_in[SEQ * j : SEQ * (j + 1), :]
    logits = l64[...]
    raised = jnp.exp(logits - jnp.max(logits, axis=-1, keepdims=True))
    rw = raised / jnp.sum(raised, axis=-1, keepdims=True)
    ids = r64[...]
    expert_of = lax.broadcasted_iota(jnp.int32, (TP * PAD, EP), 1)
    member = jnp.zeros((TP * PAD, EP), f32)
    weight = jnp.zeros((TP * PAD, EP), f32)
    for k in range(4):
        hit = ids[:, k : k + 1] == expert_of
        member = member + jnp.where(hit, 1.0, 0.0)
        weight = weight + jnp.where(hit, rw[:, k : k + 1], 0.0)
    lower = (
        lax.broadcasted_iota(jnp.int32, (TP * PAD, TP * PAD), 0)
        > lax.broadcasted_iota(jnp.int32, (TP * PAD, TP * PAD), 1)
    )
    member_b = member.astype(bf16)
    rank = mm(jnp.where(lower, 1.0, 0.0).astype(bf16), member_b)
    spread = jnp.where(
        lax.broadcasted_iota(jnp.int32, (EP, EP * CAPP), 1) // CAPP
        == lax.broadcasted_iota(jnp.int32, (EP, EP * CAPP), 0),
        1.0,
        0.0,
    ).astype(bf16)
    slot = (lax.broadcasted_iota(jnp.int32, (TP * PAD, EP * CAPP), 1) % CAPP).astype(f32)
    dt = jnp.where(
        (mm(member_b, spread) > 0.5) & (mm(rank.astype(bf16), spread) == slot), 1.0, 0.0
    )
    Dm[...] = jnp.transpose(dt).astype(bf16)
    w_hi = weight.astype(bf16)
    w_lo = (weight - w_hi.astype(f32)).astype(bf16)
    Cm[0 : TP * PAD, :] = (mm(w_hi, spread) * dt).astype(bf16)
    Cm[TP * PAD :, :] = (mm(w_lo, spread) * dt).astype(bf16)

    row = lax.broadcasted_iota(jnp.int32, (PAD, ROT), 0)
    col = lax.broadcasted_iota(jnp.int32, (PAD, ROT), 1)
    pos = jnp.zeros((PAD, ROT), f32)
    for s in range(SEQ):
        pos = jnp.where(row == s, lens[s].astype(f32), pos)
    half = ROT // 2
    freq = jnp.exp((col % half).astype(f32) * (-math.log(theta_base) / half))
    angle = pos * freq
    cosine = jnp.cos(angle)
    sine = jnp.where(col < half, -jnp.sin(angle), jnp.sin(angle))

    def rotate(v):
        swapped = jnp.concatenate([v[:, half:], v[:, :half]], axis=1)
        return v * cosine + swapped * sine

    c_wku.wait()
    c_wvu.wait()
    wtmp[0] = wku[...].astype(f32)
    wtmp[1] = wvu[...].astype(f32)
    for h in range(HL):
        wkh[h] = wtmp.at[0][pl.ds(h, LAT, stride=HL), :].astype(bf16)
        wvh[h] = wtmp.at[1][pl.ds(h, LAT, stride=HL), :].astype(bf16)

    c_wkr.wait()
    key_raw = mm(normed, wkr[...]).astype(bf16)
    new_rope = rotate(key_raw.astype(f32)).astype(bf16)
    rope_ref[...] = new_rope[0:SEQ]
    c_wq.wait()
    c_wqr.wait()
    c_wl.wait()
    for c in ph0:
        c.wait()

    rows = nbuf[...].reshape(TP * PAD, D)
    qp = mm(rows, wq[...]).astype(bf16)
    for h in range(HL):
        ql = mm_nt(qp[:, h * 128 : (h + 1) * 128], wkh[h]).astype(bf16)
        msg_s[:, :, h * LAT : (h + 1) * LAT] = ql.reshape(TP, PAD, LAT)
    msg_s[:, :, HL * LAT : HL * LAT + HL * ROT] = (
        mm(rows, wqr[...]).astype(bf16).reshape(TP, PAD, HL * ROT)
    )
    msg_s[:, :, HL * LAT + HL * ROT :] = mm(rows, wl[...]).astype(bf16).reshape(TP, PAD, 128)
    ph1 = tp_copies(1, lambda j: msg_s.at[j], msg_r.at[t])
    for c in ph1:
        c.start()
    msg_r[t] = msg_s[t]
    hl_s[...] = jnp.zeros((TP, HL, PAD, LAT), bf16)
    for c in ph1:
        c.wait()

    lat_raw = jnp.concatenate([msg_r[j, :, MSG - 128 :] for j in range(TP)], axis=1)
    new_latent = rms(lat_raw.astype(f32), g_lat[...].astype(f32)).astype(bf16)
    lat_ref[...] = new_latent[0:SEQ]
    nl32 = new_latent.astype(f32)
    nr32 = new_rope.astype(f32)
    scale = (128 + ROT) ** (-0.5)
    for j in range(TP):
        for h in range(HL):
            at = (j * HL + h) * PAD
            for c in range(LAT // 128):
                A[c, at : at + PAD, :] = msg_r[
                    j, :, h * LAT + c * 128 : h * LAT + (c + 1) * 128
                ].astype(f32)
            qr = msg_r[j, :, HL * LAT + h * ROT : HL * LAT + (h + 1) * ROT].astype(f32)
            A2[at : at + PAD, 0:ROT] = rotate(qr).astype(bf16).astype(f32)
            A2[at : at + PAD, ROT:] = jnp.zeros((PAD, 128 - ROT), f32)
    for s in range(SEQ):
        self_score = jnp.zeros((PAD, 128), f32)
        for c in range(LAT // 128):
            part = A.at[c][pl.ds(s, 16, stride=PAD), :]
            Q[s, :, c * 128 : (c + 1) * 128] = part.astype(bf16)
            self_score = self_score + part * nl32[s : s + 1, c * 128 : (c + 1) * 128]
        part = A2[pl.ds(s, 16, stride=PAD), :]
        Qr[s] = part.astype(bf16)
        total = jnp.sum(self_score, axis=-1, keepdims=True) + jnp.sum(
            part[:, 0:ROT] * nr32[s : s + 1, :], axis=-1, keepdims=True
        )
        ps_ref[s] = jnp.broadcast_to(total * scale, (16, 128))
    c_rope.wait()

    def score(s, carry):
        cache_copy(s).wait()
        val = mm_nt(Q[s], cache[s]) + mm(Qr[s, :, 0:ROT], rope[s])
        valid = lax.broadcasted_iota(jnp.int32, (16, LEN), 1) < lens[s]
        S[s] = jnp.where(valid, val * scale, -jnp.inf)
        return carry

    lax.fori_loop(0, SEQ, score, 0, unroll=2)

    def soft(s, carry):
        sc = S[s]
        own = ps_ref[s][:, 0:1]
        highest = jnp.maximum(jnp.max(sc, axis=-1, keepdims=True), own)
        e = jnp.exp(sc - highest)
        eo = jnp.exp(own - highest)
        total = jnp.sum(e, axis=-1, keepdims=True) + eo
        Pb[s] = (e / total).astype(bf16)
        ps_ref[s] = jnp.broadcast_to((eo / total).astype(bf16).astype(f32), (16, 128))
        return carry

    lax.fori_loop(0, SEQ, soft, 0, unroll=4)

    for s in range(SEQ):
        val = mm(Pb[s], cache[s]) + ps_ref[s][:, 0:1] * nl32[s : s + 1, :]
        for c in range(LAT // 128):
            O.at[c][pl.ds(s, 16, stride=PAD), :] = val[:, c * 128 : (c + 1) * 128]
    for j in range(TP):
        for h in range(HL):
            at = (j * HL + h) * PAD
            for c in range(LAT // 128):
                hl_s[j, h, 0:SEQ, c * 128 : (c + 1) * 128] = O[c, at : at + SEQ, :].astype(bf16)
    ph2 = tp_copies(2, lambda j: hl_s.at[j], hl_r.at[t])
    for c in ph2:
        c.start()
    hl_r[t] = hl_s[t]
    c_wo.wait()
    for c in ph2:
        c.wait()
    vals = jnp.concatenate(
        [mm(hl_r[:, h].reshape(TP * PAD, LAT), wvh[h]).astype(bf16) for h in range(HL)], axis=1
    )
    p_s[...] = mm(vals, wo[...]).astype(bf16).reshape(TP, PAD, D)
    ph3 = tp_copies(3, lambda j: p_s.at[j], p_r.at[t])
    for c in ph3:
        c.start()
    p_r[t] = p_s[t]
    for c in ph3:
        c.wait()
    attn = p_r[0].astype(f32)
    for j in range(1, TP):
        attn = attn + p_r[j].astype(f32)
    attn = attn.astype(bf16).astype(f32)
    mixed = (tok32[...] + rms(attn, g_post[...].astype(f32))).astype(bf16).astype(f32)
    mixed_ref[...] = mixed
    gbuf[t] = rms(mixed, g_ffn[...].astype(f32)).astype(bf16)
    ph4 = tp_copies(4, lambda j: gbuf.at[t], gbuf.at[t])
    for c in ph4:
        c.start()
    for c in (c_wg, c_wu, c_wd):
        c.wait()
    for c in ph4:
        c.wait()

    X[...] = mm(Dm[...], gbuf[...].reshape(TP * PAD, D)).astype(bf16).reshape(EP, CAPP, D)
    sent = []
    for d in far_first:
        e = ep_shift(me, d, 1)
        c = pltpu.make_async_remote_copy(
            src_ref=X.at[e],
            dst_ref=R.at[d],
            send_sem=dss.at[d],
            recv_sem=drs.at[d],
            device_id={"ep": e},
            device_id_type=MESH,
        )
        c.start()
        sent.append(c)
    R[0] = X[me]
    for c in sent:
        c.wait()
    flat = R[...].reshape(EP * CAPP, D)
    gate = jnp.minimum(mm(flat, wg[...]), clamp_limit)
    upward = jnp.clip(mm(flat, wu[...]), -clamp_limit, clamp_limit)
    active = ((upward + 1.0) * gate * jax.nn.sigmoid(sigmoid_alpha * gate)).astype(bf16)
    Y[...] = mm(active, wd[...]).astype(bf16).reshape(EP, CAPP, D)
    sent = []
    for d in far_first:
        c = pltpu.make_async_remote_copy(
            src_ref=Y.at[d],
            dst_ref=T.at[me],
            send_sem=ess.at[d],
            recv_sem=ers.at[d],
            device_id={"ep": ep_shift(me, d, -1)},
            device_id_type=MESH,
        )
        c.start()
        sent.append(c)
    T[me] = Y[0]
    for c in sent:
        c.wait()
    both = mm(Cm[...], T[...].reshape(EP * CAPP, D))
    m_s[...] = (both[0 : TP * PAD] + both[TP * PAD :]).astype(bf16).reshape(TP, PAD, D)
    ph5 = tp_copies(5, lambda j: m_s.at[j], m_r.at[t])
    for c in ph5:
        c.start()
    m_r[t] = m_s[t]
    for c in ph5:
        c.wait()
    moe = m_r[0].astype(f32)
    for j in range(1, TP):
        moe = moe + m_r[j].astype(f32)
    moe = moe.astype(bf16).astype(f32)
    res = (mixed_ref[...] + rms(moe, g_post2[...].astype(f32))).astype(bf16)
    out_ref[...] = res[0:SEQ]


def body(
    tokens,
    cache_latent,
    cache_rope,
    lengths,
    attn_gain,
    latent_gain,
    post_attn_gain,
    ffn_gain,
    post_ffn_gain,
    w_query,
    w_query_rot,
    w_latent,
    w_key_rot,
    w_key_up,
    w_value_up,
    w_out,
    route_logits,
    routes,
    w_gate,
    w_up,
    w_down,
):
    vm = pl.BlockSpec(memory_space=pltpu.VMEM)
    hbm = pl.BlockSpec(memory_space=pl.ANY)
    V = pltpu.VMEM
    scratch = [
        V((PAD, D), f32),
        V((TP, PAD, D), bf16),
        V((D, 512), bf16),
        V((D, 256), bf16),
        V((D, 128), bf16),
        V((D, ROT), bf16),
        V((HL * LAT, 128), bf16),
        V((HL * LAT, 128), bf16),
        V((2, HL * LAT, 128), f32),
        V((HL, LAT, 128), bf16),
        V((HL, LAT, 128), bf16),
        V((TP, PAD, MSG), bf16),
        V((TP, PAD, MSG), bf16),
        V((SEQ, LEN, LAT), bf16),
        V((SEQ, ROT, LEN), bf16),
        V((LAT // 128, 256, 128), f32),
        V((256, 128), f32),
        V((SEQ, 16, LAT), bf16),
        V((SEQ, 16, 128), bf16),
        V((SEQ, 16, LEN), f32),
        V((SEQ, 16, LEN), bf16),
        V((SEQ, 16, 128), f32),
        V((LAT // 128, 256, 128), f32),
        V((TP, HL, PAD, LAT), bf16),
        V((TP, HL, PAD, LAT), bf16),
        V((512, D), bf16),
        V((TP, PAD, D), bf16),
        V((TP, PAD, D), bf16),
        V((TP, PAD, D), bf16),
        V((PAD, D), f32),
        V((TP * PAD, 4), jnp.int32),
        V((TP * PAD, 4), f32),
        V((EP * CAPP, TP * PAD), bf16),
        V((2 * TP * PAD, EP * CAPP), bf16),
        V((EP, CAPP, D), bf16),
        V((EP, CAPP, D), bf16),
        V((EP, CAPP, D), bf16),
        V((EP, CAPP, D), bf16),
        V((D, 512), bf16),
        V((D, 512), bf16),
        V((512, D), bf16),
        V((TP, PAD, D), bf16),
        V((TP, PAD, D), bf16),
        pltpu.SemaphoreType.DMA((10,)),
        pltpu.SemaphoreType.DMA((SEQ,)),
        pltpu.SemaphoreType.DMA,
        pltpu.SemaphoreType.DMA((6, 4)),
        pltpu.SemaphoreType.DMA((6, 4)),
        pltpu.SemaphoreType.DMA((EP,)),
        pltpu.SemaphoreType.DMA((EP,)),
        pltpu.SemaphoreType.DMA((EP,)),
        pltpu.SemaphoreType.DMA((EP,)),
    ]
    return pl.pallas_call(
        layer_kernel,
        name="layer",
        out_shape=(
            jax.ShapeDtypeStruct((SEQ, D), bf16),
            jax.ShapeDtypeStruct((SEQ, LAT), bf16),
            jax.ShapeDtypeStruct((SEQ, ROT), bf16),
        ),
        in_specs=[pl.BlockSpec(memory_space=pltpu.SMEM)] + [vm] * 8 + [hbm] * 12,
        out_specs=(vm, vm, vm),
        scratch_shapes=scratch,
        compiler_params=pltpu.CompilerParams(
            collective_id=0, has_side_effects=True, vmem_limit_bytes=60 * 1024 * 1024
        ),
    )(
        lengths,
        tokens,
        routes,
        route_logits,
        attn_gain.reshape(1, -1),
        latent_gain.reshape(1, -1),
        post_attn_gain.reshape(1, -1),
        ffn_gain.reshape(1, -1),
        post_ffn_gain.reshape(1, -1),
        cache_latent,
        cache_rope,
        w_query,
        w_query_rot,
        w_latent,
        w_key_rot,
        w_key_up.reshape(-1, w_key_up.shape[2]),
        w_value_up.reshape(-1, w_value_up.shape[2]),
        w_out,
        w_gate,
        w_up,
        w_down,
    )


def solution(mesh):
    return jax.shard_map(
        body,
        mesh=mesh,
        in_specs=(
            P(("ep", "tp"), None),
            P(("ep", "tp"), None, None),
            P(("ep", "tp"), None, None),
            P(("ep", "tp")),
            P(),
            P(),
            P(),
            P(),
            P(),
            P(None, "tp"),
            P(None, "tp"),
            P(None, "tp"),
            P(),
            P(None, "tp", None),
            P(None, "tp", None),
            P("tp", None),
            P("ep", None),
            P("ep", None),
            P("ep", None, "tp"),
            P("ep", None, "tp"),
            P("ep", "tp", None),
        ),
        out_specs=(P(("ep", "tp"), None), P(("ep", "tp"), None), P(("ep", "tp"), None)),
        check_vma=False,
    )
```

time: 172 us -> 94.9 us (0.55)
  Pallas kernels: 0 us -> 78.6 us
  waiting for transfers between devices: 49.6 us -> 0 us
  starting transfers between devices: 41.7 us -> 0 us
  blocking collectives: 33.4 us -> 0 us
  matrix products: 21.8 us -> 0 us
  other arithmetic: 11.1 us -> 0 us
  local copies, waits for them, and re-layouts: 11.4 us -> 15.1 us
    pallas_call x0 -> x1, Pallas kernels: none -> 78.6 us  [body(): pl.pallas_call(layer_kernel, name='layer', out_shape=(jax.ShapeDtypeStruc...]
    all_to_all x9 -> x0, waiting for transfers between devices: 49.6 us -> none  [the longest x2 18.5 us: sum_at_owner(): lax.all_to_all(parts, axis, split_axis=0, concat_axis=0, tiled=True)]
    all_to_all x9 -> x0, starting transfers between devices: 41.7 us -> none  [the longest x1 10.8 us: body(): lax.all_to_all(head_latent, 'tp', split_axis=1, concat_axis=0, tiled=True)]
    all_to_all x1 -> x0, blocking collectives: 33.4 us -> none  [body(): lax.all_to_all(slots, 'ep', split_axis=0, concat_axis=0, tiled=True)]
    dot_general x15 -> x0, matrix products: 21.8 us -> none  [the longest x1 4.65 us: score_block(): jnp.einsum('shc,spc->shp', query_latent, latents, preferred_element_type=...]
    unnamed x25 -> x6, local copies, waits for them, and re-layouts: 0.93 us -> 8.75 us
    convert_element_type x16 -> x0, other arithmetic: 5.96 us -> none  [the longest x5 1.53 us: rms_scale(): return values * lax.rsqrt(mean_square + eps_norm) * gain.astype(jnp.float32)]
    reduce_sum x11 -> x0, other arithmetic: 2.23 us -> none  [the longest x5 1.56 us: rms_scale(): mean_square = jnp.mean(values * values, axis=-1, keepdims=True)]
  transfers between devices with their start and end apart: 9 -> 0, of which waited for: 8 -> 0; matrix products, arithmetic and copies ran while one was open for 5% -> 0% of each run, Pallas kernels for 0% -> 0%
where the time goes in v1:
time: 94.9 us; the launch traced here: 94.3 us
  Pallas kernels  78.6 us (83%)
  local copies, waits for them, and re-layouts  15.1 us (16%)
    pallas_call x1, Pallas kernels, body(): pl.pallas_call(layer_kernel, name='layer', out_shape=(jax.ShapeDtypeStruc...  78.6 us
    unnamed x6, local copies, waits for them, and re-layouts  8.75 us

profile of v1, /device:TPU:1, one launch (start us, length us, event | category | flops | bytes accessed | tf_op | source)
XLA Modules:
  0.0 94.3 jit_solution(12500539827143449259)
XLA Ops:
  0.6 1.3 %reshape.28.g_lat = bf16[1,512]{1,0:T(2,128)(2,1)} reshape(bf16[512]{0:T(512)(128)(2,1)} %param.26) | data formatting | bytes 2048 | tf_op jit(solution)/shard_map/reshape | solution.py:531
  1.9 1.3 %reshape.27.g_attn = bf16[1,2048]{1,0:T(2,128)(2,1)} reshape(bf16[2048]{0:T(1024)(128)(2,1)} %param.25) | data formatting | bytes 8192 | tf_op jit(solution)/shard_map/reshape | solution.py:530
  3.2 1.3 %reshape.29.g_post = bf16[1,2048]{1,0:T(2,128)(2,1)} reshape(bf16[2048]{0:T(1024)(128)(2,1)} %param.27) | data formatting | bytes 8192 | tf_op jit(solution)/shard_map/reshape | solution.py:532
  4.4 1.3 %reshape.30.g_ffn = bf16[1,2048]{1,0:T(2,128)(2,1)} reshape(bf16[2048]{0:T(1024)(128)(2,1)} %param.28) | data formatting | bytes 8192 | tf_op jit(solution)/shard_map/reshape | solution.py:533
  5.7 1.3 %reshape.31.g_post2 = bf16[1,2048]{1,0:T(2,128)(2,1)} reshape(bf16[2048]{0:T(1024)(128)(2,1)} %param.29) | data formatting | bytes 8192 | tf_op jit(solution)/shard_map/reshape | solution.py:534
  7.0 1.4 %copy.25.logits_in = f32[48,4]{1,0:T(8,128)} copy(f32[48,4]{0,1:T(4,128)} %param.37) | data formatting | bytes 1536 | tf_op args[16]
  8.4 1.4 %copy.24.routes_in = s32[48,4]{1,0:T(8,128)} copy(s32[48,4]{0,1:T(4,128)} %param.38) | data formatting | bytes 1536 | tf_op args[17]
  9.8 1.9 %copy.26.h_wkr = bf16[2048,64]{1,0:T(8,128)(2,1)} copy(bf16[2048,64]{0,1:T(8,128)(2,1)} %param.33) | data formatting | bytes 524288 | tf_op args[12]
  11.7 78.6 %layer.1 = (bf16[12,2048]{1,0:T(8,128)(2,1)}, bf16[12,512]{1,0:T(8,128)(2,1)}, bf16[12,64]{1,0:T(8,128)(2,1)}) custom-call(s32[12]{0:T(128)} %lens.1, bf16[12,2048]{1,0:T(8,128)(2,1)} %tok_in.1, s32[48,4]{1,0:T(8,128)} %copy.24.routes_in, f32[48,4]{1,0:T(8,128)} %copy.25.logits_in, bf16[1,2048]{1,0:T(2,128)(2,1)} %reshape.27.g_attn, ...), custom_call_target="tpu_custom_call" | custom-call | tf_op jit(solution)/shard_map/layer/pallas_call | solution.py:511
  90.3 1.5 %copy.30 = bf16[12,2048]{1,0:T(8,128)(2,1)} copy(bf16[12,2048]{1,0:T(8,128)(2,1)} %get-tuple-element.6) | data formatting | bytes 98304
  91.7 1.3 %copy.31 = bf16[12,512]{1,0:T(8,128)(2,1)} copy(bf16[12,512]{1,0:T(8,128)(2,1)} %get-tuple-element.7) | data formatting | bytes 24576
  93.1 1.3 %copy.32 = bf16[12,64]{1,0:T(8,128)(2,1)} copy(bf16[12,64]{1,0:T(8,128)(2,1)} %get-tuple-element.8) | data formatting | bytes 3072

commit v2 on v1

v2 whole, which is shorter than its diff:
```python
import functools
import math

import jax
import jax.numpy as jnp
from jax import lax
from jax.experimental import pallas as pl
from jax.experimental.pallas import tpu as pltpu
from jax.sharding import PartitionSpec as P

MESH = pl.DeviceIdType.MESH
eps_norm = 1e-06
clamp_limit = 7.0
sigmoid_alpha = 1.702
theta_base = 10000.0
f32 = jnp.float32
bf16 = jnp.bfloat16

SEQ = 12
PAD = 12
D = 2048
LAT = 512
ROT = 64
LEN = 1024
HL = 4
TP = 4
EP = 32
CAPP = 8
MSG = HL * LAT + HL * ROT + 128


def hops(a):
    return min(a, 4 - a)


far_first = sorted(range(1, EP), key=lambda d: -(hops(d // 8) + hops((d // 2) % 4)))


order = far_first + [0]
CHUNK = 16


def ep_shift(me, d, sign):
    z, y, c = me // 8, (me // 2) % 4, me % 2
    dz, dy, dc = d // 8, (d // 2) % 4, d % 2
    if sign < 0:
        dz, dy = (4 - dz) % 4, (4 - dy) % 4
    return ((z + dz) % 4) * 8 + ((y + dy) % 4) * 2 + (c + dc) % 2


def mm(a, b):
    return lax.dot_general(a, b, (((1,), (0,)), ((), ())), preferred_element_type=f32)


def mm_nt(a, b):
    return lax.dot_general(a, b, (((1,), (1,)), ((), ())), preferred_element_type=f32)


def rms(v, gain):
    mean_square = jnp.mean(v * v, axis=-1, keepdims=True)
    return v * lax.rsqrt(mean_square + eps_norm) * gain


def layer_kernel(
    h_lens,
    h_tok,
    h_routes,
    h_logits,
    h_attn,
    h_lat,
    h_post,
    h_ffn,
    h_post2,
    h_clat,
    h_crope,
    h_wq,
    h_wqr,
    h_wl,
    h_wkr,
    h_wku,
    h_wvu,
    h_wo,
    h_wg,
    h_wu,
    h_wd,
    out_ref,
    lat_ref,
    rope_ref,
    lens,
    tok_in,
    routes_in,
    logits_in,
    g_attn,
    g_lat,
    g_post,
    g_ffn,
    g_post2,
    tok32,
    nbuf,
    wq,
    wqr,
    wl,
    wkr,
    wku,
    wvu,
    wtmp,
    wkh,
    wvh,
    msg_s,
    msg_r,
    cache,
    rope,
    A,
    A2,
    Q,
    Qr,
    S,
    Pb,
    ps_ref,
    O,
    hl_s,
    hl_r,
    wo,
    p_s,
    p_r,
    gbuf,
    mixed_ref,
    Dm,
    Cm,
    X,
    R,
    Y,
    T,
    wg,
    wu,
    wd,
    m_s,
    m_r,
    lsem,
    csem,
    rsem,
    tss,
    trs,
    dss,
    drs,
    ess,
    ers,
):
    me = lax.axis_index("ep")
    t = lax.axis_index("tp")
    barrier = pltpu.get_barrier_semaphore()
    for d in (1, 2, 3):
        pl.semaphore_signal(barrier, inc=1, device_id={"tp": (t + d) % TP}, device_id_type=MESH)
    for d in far_first:
        pl.semaphore_signal(barrier, inc=1, device_id={"ep": ep_shift(me, d, 1)}, device_id_type=MESH)

    def local(src, dst, i):
        return pltpu.make_async_copy(src, dst, lsem.at[i])

    c_wq = local(h_wq, wq, 0)
    c_wqr = local(h_wqr, wqr, 1)
    c_wl = local(h_wl, wl, 2)
    c_wkr = local(h_wkr, wkr, 3)
    c_wku = local(h_wku, wku, 4)
    c_wvu = local(h_wvu, wvu, 5)
    c_wo = local(h_wo, wo, 6)
    c_wg = local(h_wg.at[0], wg, 7)
    c_wu = local(h_wu.at[0], wu, 8)
    c_wd = local(h_wd.at[0], wd, 9)
    c_tok = local(h_tok, tok_in, 10)
    c_attn = local(h_attn, g_attn, 11)
    c_lens = local(h_lens, lens, 12)
    c_routes = local(h_routes, routes_in, 13)
    c_logits = local(h_logits, logits_in, 14)
    c_lat = local(h_lat, g_lat, 15)
    c_post = local(h_post, g_post, 16)
    c_ffn = local(h_ffn, g_ffn, 17)
    c_post2 = local(h_post2, g_post2, 18)
    small = (c_lens, c_routes, c_logits, c_lat, c_post, c_ffn, c_post2)
    for c in (c_tok, c_attn) + small + (c_wku, c_wvu, c_wq, c_wqr, c_wl, c_wkr):
        c.start()

    def cache_copy(s):
        return pltpu.make_async_copy(h_clat.at[s], cache.at[s], csem.at[s])

    c_rope = pltpu.make_async_copy(h_crope, rope, rsem)

    c_rope.start()
    for s in range(SEQ):
        cache_copy(s).start()

    def tp_copies(phase, src, dst):
        out = []
        for d in (2, 1, 3):
            j = (t + d) % TP
            out.append(
                pltpu.make_async_remote_copy(
                    src_ref=src(j),
                    dst_ref=dst,
                    send_sem=tss.at[phase, d],
                    recv_sem=trs.at[phase, d],
                    device_id={"tp": j},
                    device_id_type=MESH,
                )
            )
        return out

    c_tok.wait()
    c_attn.wait()
    tok32[...] = tok_in[...].astype(f32)
    normed = rms(tok32[...], g_attn[...].astype(f32)).astype(bf16)
    nbuf[t] = normed.reshape(3, 4, D)
    with jax.named_scope("wait_barrier"):
        pl.semaphore_wait(barrier, 34)
    ph0 = tp_copies(0, lambda j: nbuf.at[t], nbuf.at[t])
    for c in ph0:
        c.start()

    for c in small:
        c.wait()

    logits = logits_in[...]
    raised = jnp.exp(logits - jnp.max(logits, axis=0, keepdims=True))
    rw = raised / jnp.sum(raised, axis=0, keepdims=True)
    ids = routes_in[...]
    expert_of = lax.broadcasted_iota(jnp.int32, (EP, TP * PAD), 0)
    member = jnp.zeros((EP, TP * PAD), f32)
    weight = jnp.zeros((EP, TP * PAD), f32)
    for k in range(4):
        hit = ids[k : k + 1, :] == expert_of
        member = member + jnp.where(hit, 1.0, 0.0)
        weight = weight + jnp.where(hit, rw[k : k + 1, :], 0.0)
    earlier = (
        lax.broadcasted_iota(jnp.int32, (TP * PAD, TP * PAD), 0)
        < lax.broadcasted_iota(jnp.int32, (TP * PAD, TP * PAD), 1)
    )
    member_b = member.astype(bf16)
    rank = mm(member_b, jnp.where(earlier, 1.0, 0.0).astype(bf16))
    spread = jnp.where(
        lax.broadcasted_iota(jnp.int32, (EP * CAPP, EP), 0) // CAPP
        == lax.broadcasted_iota(jnp.int32, (EP * CAPP, EP), 1),
        1.0,
        0.0,
    ).astype(bf16)
    slot = (lax.broadcasted_iota(jnp.int32, (EP * CAPP, TP * PAD), 0) % CAPP).astype(f32)
    dm = jnp.where(
        (mm(spread, member_b) > 0.5) & (mm(spread, rank.astype(bf16)) == slot), 1.0, 0.0
    )
    Dm[...] = dm.astype(bf16)
    w_hi = weight.astype(bf16)
    w_lo = (weight - w_hi.astype(f32)).astype(bf16)
    Cm[0 : TP * PAD, :] = jnp.transpose(mm(spread, w_hi) * dm).astype(bf16)
    Cm[TP * PAD :, :] = jnp.transpose(mm(spread, w_lo) * dm).astype(bf16)

    row = lax.broadcasted_iota(jnp.int32, (PAD, ROT), 0)
    col = lax.broadcasted_iota(jnp.int32, (PAD, ROT), 1)
    pos = jnp.zeros((PAD, ROT), f32)
    for s in range(SEQ):
        pos = jnp.where(row == s, lens[s].astype(f32), pos)
    half = ROT // 2
    freq = jnp.exp((col % half).astype(f32) * (-math.log(theta_base) / half))
    angle = pos * freq
    cosine = jnp.cos(angle)
    sine = jnp.where(col < half, -jnp.sin(angle), jnp.sin(angle))

    def rotate(v):
        swapped = jnp.concatenate([v[:, half:], v[:, :half]], axis=1)
        return v * cosine + swapped * sine

    with jax.named_scope("wait_up"):
        c_wku.wait()
        c_wvu.wait()
    wtmp[0] = wku[...].astype(f32)
    wtmp[1] = wvu[...].astype(f32)
    for h in range(HL):
        wkh[h] = wtmp.at[0][pl.ds(h, LAT, stride=HL), :].astype(bf16)
        wvh[h] = wtmp.at[1][pl.ds(h, LAT, stride=HL), :].astype(bf16)

    c_wkr.wait()
    key_raw = mm_nt(normed, wkr[...]).astype(bf16)
    new_rope = rotate(key_raw.astype(f32)).astype(bf16)
    rope_ref[...] = new_rope
    with jax.named_scope("wait_wq"):
        c_wq.wait()
        c_wqr.wait()
        c_wl.wait()
    with jax.named_scope("wait_tp0"):
        for c in ph0:
            c.wait()

    rows = nbuf[...].reshape(TP * PAD, D)
    qp = mm(rows, wq[...]).astype(bf16)
    for h in range(HL):
        ql = mm_nt(qp[:, h * 128 : (h + 1) * 128], wkh[h]).astype(bf16)
        msg_s[:, :, :, h * LAT : (h + 1) * LAT] = ql.reshape(TP, 3, 4, LAT)
    msg_s[:, :, :, HL * LAT : HL * LAT + HL * ROT] = (
        mm(rows, wqr[...]).astype(bf16).reshape(TP, 3, 4, HL * ROT)
    )
    msg_s[:, :, :, HL * LAT + HL * ROT :] = (
        mm(rows, wl[...]).astype(bf16).reshape(TP, 3, 4, 128)
    )
    ph1 = tp_copies(1, lambda j: msg_s.at[j], msg_r.at[t])
    for c in ph1:
        c.start()
    msg_r[t] = msg_s[t]
    with jax.named_scope("wait_tp1"):
        for c in ph1:
            c.wait()

    lat_raw = jnp.concatenate([msg_r[j, :, :, MSG - 128 :].reshape(PAD, 128) for j in range(TP)], axis=1)
    new_latent = rms(lat_raw.astype(f32), g_lat[...].astype(f32)).astype(bf16)
    lat_ref[...] = new_latent
    nl32 = new_latent.astype(f32)
    nr32 = new_rope.astype(f32)
    scale = (128 + ROT) ** (-0.5)
    for j in range(TP):
        for h in range(HL):
            at = (j * HL + h) * PAD
            for c in range(LAT // 128):
                A[c, at : at + PAD, :] = (
                    msg_r[j, :, :, h * LAT + c * 128 : h * LAT + (c + 1) * 128]
                    .reshape(PAD, 128)
                    .astype(f32)
                )
            qr = (
                msg_r[j, :, :, HL * LAT + h * ROT : HL * LAT + (h + 1) * ROT]
                .reshape(PAD, ROT)
                .astype(f32)
            )
            A2[at : at + PAD, 0:ROT] = rotate(qr).astype(bf16).astype(f32)
            A2[at : at + PAD, ROT:] = jnp.zeros((PAD, 128 - ROT), f32)
    for s in range(SEQ):
        self_score = jnp.zeros((16, 128), f32)
        for c in range(LAT // 128):
            part = A.at[c][pl.ds(s, 16, stride=PAD), :]
            Q[s, :, c * 128 : (c + 1) * 128] = part.astype(bf16)
            self_score = self_score + part * nl32[s : s + 1, c * 128 : (c + 1) * 128]
        part = A2[pl.ds(s, 16, stride=PAD), :]
        Qr[s] = part.astype(bf16)
        total = jnp.sum(self_score, axis=-1, keepdims=True) + jnp.sum(
            part[:, 0:ROT] * nr32[s : s + 1, :], axis=-1, keepdims=True
        )
        ps_ref[s] = jnp.broadcast_to(total * scale, (16, 128))
    c_rope.wait()

    def score(s, carry):
        cache_copy(s).wait()
        val = mm_nt(Q[s], cache[s]) + mm(Qr[s, :, 0:ROT], rope[s])
        valid = lax.broadcasted_iota(jnp.int32, (16, LEN), 1) < lens[s]
        S[s] = jnp.where(valid, val * scale, -jnp.inf)
        return carry

    with jax.named_scope("scores"):
        lax.fori_loop(0, SEQ, score, 0, unroll=2)

    def soft(s, carry):
        sc = S[s]
        own = ps_ref[s][:, 0:1]
        highest = jnp.maximum(jnp.max(sc, axis=-1, keepdims=True), own)
        e = jnp.exp(sc - highest)
        eo = jnp.exp(own - highest)
        total = jnp.sum(e, axis=-1, keepdims=True) + eo
        Pb[s] = (e / total).astype(bf16)
        ps_ref[s] = jnp.broadcast_to((eo / total).astype(bf16).astype(f32), (16, 128))
        return carry

    for c in (c_wo, c_wg, c_wu, c_wd):
        c.start()
    with jax.named_scope("softmax"):
        lax.fori_loop(0, SEQ, soft, 0, unroll=4)

    for s in range(SEQ):
        val = mm(Pb[s], cache[s]) + ps_ref[s][:, 0:1] * nl32[s : s + 1, :]
        for c in range(LAT // 128):
            O.at[c][pl.ds(s, 16, stride=PAD), :] = val[:, c * 128 : (c + 1) * 128]
    for j in range(TP):
        for h in range(HL):
            at = (j * HL + h) * PAD
            for c in range(LAT // 128):
                hl_s[j, h, :, :, c * 128 : (c + 1) * 128] = (
                    O[c, at : at + PAD, :].astype(bf16).reshape(3, 4, 128)
                )
    ph2 = tp_copies(2, lambda j: hl_s.at[j], hl_r.at[t])
    for c in ph2:
        c.start()
    hl_r[t] = hl_s[t]
    c_wo.wait()
    with jax.named_scope("wait_tp2"):
        for c in ph2:
            c.wait()
    vals = jnp.concatenate(
        [mm(hl_r[:, h].reshape(TP * PAD, LAT), wvh[h]).astype(bf16) for h in range(HL)], axis=1
    )
    p_s[...] = mm(vals, wo[...]).astype(bf16).reshape(TP, 3, 4, D)
    ph3 = tp_copies(3, lambda j: p_s.at[j], p_r.at[t])
    for c in ph3:
        c.start()
    p_r[t] = p_s[t]
    with jax.named_scope("wait_tp3"):
        for c in ph3:
            c.wait()
    attn = p_r[0].reshape(PAD, D).astype(f32)
    for j in range(1, TP):
        attn = attn + p_r[j].reshape(PAD, D).astype(f32)
    attn = attn.astype(bf16).astype(f32)
    mixed = (tok32[...] + rms(attn, g_post[...].astype(f32))).astype(bf16).astype(f32)
    mixed_ref[...] = mixed
    gbuf[t] = rms(mixed, g_ffn[...].astype(f32)).astype(bf16).reshape(3, 4, D)
    ph4 = tp_copies(4, lambda j: gbuf.at[t], gbuf.at[t])
    for c in ph4:
        c.start()
    for c in (c_wg, c_wu, c_wd):
        c.wait()
    with jax.named_scope("wait_tp4"):
        for c in ph4:
            c.wait()

    X[...] = mm(Dm[...], gbuf[...].reshape(TP * PAD, D)).astype(bf16).reshape(EP, CAPP, D)
    for p, d in enumerate(order):
        if d:
            e = ep_shift(me, d, 1)
            pltpu.make_async_remote_copy(
                src_ref=X.at[e],
                dst_ref=R.at[p],
                send_sem=dss,
                recv_sem=drs.at[p // CHUNK],
                device_id={"ep": e},
                device_id_type=MESH,
            ).start()
        else:
            R[p] = X[me]

    def arrived(ref, sem):
        pltpu.make_async_copy(ref, ref, sem).wait()

    for k in range(EP // CHUNK):
        lo, hi = k * CHUNK, (k + 1) * CHUNK
        with jax.named_scope(f"wait_dispatch{k}"):
            arrived(R.at[lo : min(hi, EP - 1)], drs.at[k])
        flat = R[lo:hi].reshape(CHUNK * CAPP, D)
        gate = jnp.minimum(mm(flat, wg[...]), clamp_limit)
        upward = jnp.clip(mm(flat, wu[...]), -clamp_limit, clamp_limit)
        active = ((upward + 1.0) * gate * jax.nn.sigmoid(sigmoid_alpha * gate)).astype(bf16)
        Y[lo:hi] = mm(active, wd[...]).astype(bf16).reshape(CHUNK, CAPP, D)
        for p in range(lo, hi):
            d = order[p]
            if d:
                pltpu.make_async_remote_copy(
                    src_ref=Y.at[p],
                    dst_ref=T.at[me],
                    send_sem=ess,
                    recv_sem=ers,
                    device_id={"ep": ep_shift(me, d, -1)},
                    device_id_type=MESH,
                ).start()
            else:
                T[me] = Y[p]
    with jax.named_scope("wait_return"):
        arrived(T.at[0 : EP - 1], ers)
    both = mm(Cm[...], T[...].reshape(EP * CAPP, D))
    m_s[...] = (both[0 : TP * PAD] + both[TP * PAD :]).astype(bf16).reshape(TP, 3, 4, D)
    ph5 = tp_copies(5, lambda j: m_s.at[j], m_r.at[t])
    for c in ph5:
        c.start()
    m_r[t] = m_s[t]
    with jax.named_scope("wait_tp5"):
        for c in ph5:
            c.wait()
    with jax.named_scope("final"):
      moe = m_r[0].reshape(PAD, D).astype(f32)
      for j in range(1, TP):
        moe = moe + m_r[j].reshape(PAD, D).astype(f32)
      moe = moe.astype(bf16).astype(f32)
      arrived(X.at[0 : EP - 1], dss)
      arrived(Y.at[0 : EP - 1], ess)
      res = (mixed_ref[...] + rms(moe, g_post2[...].astype(f32))).astype(bf16)
      out_ref[...] = res


def finish_kernel(a, b, c, x, y, z, sem):
    copies = [pltpu.make_async_copy(p, q, sem.at[i]) for i, (p, q) in enumerate(((a, x), (b, y), (c, z)))]
    for p in copies:
        p.start()
    for p in copies:
        p.wait()


def body(
    tokens,
    cache_latent,
    cache_rope,
    lengths,
    attn_gain,
    latent_gain,
    post_attn_gain,
    ffn_gain,
    post_ffn_gain,
    w_query,
    w_query_rot,
    w_latent,
    w_key_rot,
    w_key_up,
    w_value_up,
    w_out,
    route_logits,
    routes,
    w_gate,
    w_up,
    w_down,
):
    vm = pl.BlockSpec(memory_space=pltpu.VMEM)
    hbm = pl.BlockSpec(memory_space=pl.ANY)
    V = pltpu.VMEM
    scratch = [
        pltpu.SMEM((SEQ,), jnp.int32),
        V((SEQ, D), bf16),
        V((4, TP * SEQ), jnp.int32),
        V((4, TP * SEQ), f32),
        V((D,), bf16),
        V((LAT,), bf16),
        V((D,), bf16),
        V((D,), bf16),
        V((D,), bf16),
        V((PAD, D), f32),
        V((TP, 3, 4, D), bf16),
        V((D, 512), bf16),
        V((D, 256), bf16),
        V((D, 128), bf16),
        V((ROT, D), bf16),
        V((HL * LAT, 128), bf16),
        V((HL * LAT, 128), bf16),
        V((2, HL * LAT, 128), f32),
        V((HL, LAT, 128), bf16),
        V((HL, LAT, 128), bf16),
        V((TP, 3, 4, MSG), bf16),
        V((TP, 3, 4, MSG), bf16),
        V((SEQ, LEN, LAT), bf16),
        V((SEQ, ROT, LEN), bf16),
        V((LAT // 128, 16 * PAD, 128), f32),
        V((16 * PAD, 128), f32),
        V((SEQ, 16, LAT), bf16),
        V((SEQ, 16, 128), bf16),
        V((SEQ, 16, LEN), f32),
        V((SEQ, 16, LEN), bf16),
        V((SEQ, 16, 128), f32),
        V((LAT // 128, 16 * PAD, 128), f32),
        V((TP, HL, 3, 4, LAT), bf16),
        V((TP, HL, 3, 4, LAT), bf16),
        V((512, D), bf16),
        V((TP, 3, 4, D), bf16),
        V((TP, 3, 4, D), bf16),
        V((TP, 3, 4, D), bf16),
        V((PAD, D), f32),
        V((EP * CAPP, TP * PAD), bf16),
        V((2 * TP * PAD, EP * CAPP), bf16),
        V((EP, CAPP, D), bf16),
        V((EP, CAPP, D), bf16),
        V((EP, CAPP, D), bf16),
        V((EP, CAPP, D), bf16),
        V((D, 512), bf16),
        V((D, 512), bf16),
        V((512, D), bf16),
        V((TP, 3, 4, D), bf16),
        V((TP, 3, 4, D), bf16),
        pltpu.SemaphoreType.DMA((19,)),
        pltpu.SemaphoreType.DMA((SEQ,)),
        pltpu.SemaphoreType.DMA,
        pltpu.SemaphoreType.DMA((6, 4)),
        pltpu.SemaphoreType.DMA((6, 4)),
        pltpu.SemaphoreType.DMA,
        pltpu.SemaphoreType.DMA((EP // CHUNK,)),
        pltpu.SemaphoreType.DMA,
        pltpu.SemaphoreType.DMA,
    ]
    parts = pl.pallas_call(
        layer_kernel,
        name="layer",
        out_shape=(
            pltpu.VMEM((SEQ, D), bf16),
            pltpu.VMEM((SEQ, LAT), bf16),
            pltpu.VMEM((SEQ, ROT), bf16),
        ),
        in_specs=[hbm] * 21,
        out_specs=(vm, vm, vm),
        scratch_shapes=scratch,
        compiler_params=pltpu.CompilerParams(
            collective_id=0, has_side_effects=True, vmem_limit_bytes=60 * 1024 * 1024
        ),
    )(
        lengths,
        tokens,
        routes.T,
        route_logits.T,
        attn_gain,
        latent_gain,
        post_attn_gain,
        ffn_gain,
        post_ffn_gain,
        cache_latent,
        cache_rope,
        w_query,
        w_query_rot,
        w_latent,
        w_key_rot.T,
        w_key_up.reshape(-1, w_key_up.shape[2]),
        w_value_up.reshape(-1, w_value_up.shape[2]),
        w_out,
        w_gate,
        w_up,
        w_down,
    )
    parts = [pltpu.with_memory_space_constraint(p, pltpu.VMEM) for p in parts]
    return pl.pallas_call(
        finish_kernel,
        name="finish",
        out_shape=(
            jax.ShapeDtypeStruct((SEQ, D), bf16),
            jax.ShapeDtypeStruct((SEQ, LAT), bf16),
            jax.ShapeDtypeStruct((SEQ, ROT), bf16),
        ),
        in_specs=[vm] * 3,
        out_specs=(hbm,) * 3,
        scratch_shapes=[pltpu.SemaphoreType.DMA((3,))],
    )(*parts)


def solution(mesh):
    return jax.shard_map(
        body,
        mesh=mesh,
        in_specs=(
            P(("ep", "tp"), None),
            P(("ep", "tp"), None, None),
            P(("ep", "tp"), None, None),
            P(("ep", "tp")),
            P(),
            P(),
            P(),
            P(),
            P(),
            P(None, "tp"),
            P(None, "tp"),
            P(None, "tp"),
            P(),
            P(None, "tp", None),
            P(None, "tp", None),
            P("tp", None),
            P("ep", None),
            P("ep", None),
            P("ep", None, "tp"),
            P("ep", None, "tp"),
            P("ep", "tp", None),
        ),
        out_specs=(P(("ep", "tp"), None), P(("ep", "tp"), None), P(("ep", "tp"), None)),
        check_vma=False,
    )
```

time: 94.9 us -> 73.3 us (0.77)
  local copies, waits for them, and re-layouts: 15.1 us -> 0 us
  Pallas kernels: 78.6 us -> 72.5 us
    unnamed x6 -> x0, local copies, waits for them, and re-layouts: 8.75 us -> none
    reshape x5 -> x0, local copies, waits for them, and re-layouts: 6.39 us -> none  [the longest x1 1.29 us: body(): attn_gain.reshape(1, -1)]
    pallas_call x1 -> x2, Pallas kernels: 78.6 us -> 72.5 us  [the longest x1 71.9 us: body(): pl.pallas_call(layer_kernel, name='layer', out_shape=(pltpu.VMEM((SEQ, D)...]
where the time goes in v2:
time: 73.3 us; the launch traced here: 73.2 us
  Pallas kernels  72.5 us (99%)
    pallas_call x1, Pallas kernels, body(): pl.pallas_call(layer_kernel, name='layer', out_shape=(pltpu.VMEM((SEQ, D)...  71.9 us

profile of v2, /device:TPU:1, one launch (start us, length us, event | category | flops | bytes accessed | tf_op | source)
XLA Modules:
  0.0 73.2 jit_solution(16014100155656630385)
XLA Ops:
  0.6 71.9 %layer.1 = (bf16[12,2048]{1,0:T(8,128)(2,1)S(1)}, bf16[12,512]{1,0:T(8,128)(2,1)S(1)}, bf16[12,64]{1,0:T(8,128)(2,1)S(1)}) custom-call(s32[12]{0:T(128)} %h_lens.1, bf16[12,2048]{1,0:T(8,128)(2,1)} %h_tok.1, s32[4,48]{1,0:T(4,128)} %bitcast.8, f32[4,48]{1,0:T(4,128)} %bitcast.9, bf16[2048]{0:T(1024)(128)(2,1)} %h_attn.1, bf16[512]{0:T(512)(128)(2,1)} %h_lat.1, ...), custom_call_target="tpu_custom_call" | custom-call | tf_op jit(solution)/shard_map/layer/pallas_call | solution.py:575
  72.5 0.7 finish.1

commit v3 on v2

--- a/solution.py
+++ b/solution.py
@@ -109,6 +109,7 @@
     msg_s,
     msg_r,
     cache,
+    turned,
     rope,
     A,
     A2,
@@ -141,6 +142,8 @@
     rsem,
     tss,
     trs,
+    hss,
+    hrs,
     dss,
     drs,
     ess,
@@ -189,6 +192,13 @@
     for s in range(SEQ):
         cache_copy(s).start()
 
+    def arrived(ref, sem):
+        pltpu.make_async_copy(ref, ref, sem).wait()
+
+    def turn(s):
+        cache_copy(s).wait()
+        turned[s] = cache[s].T
+
     def tp_copies(phase, src, dst):
         out = []
         for d in (2, 1, 3):
@@ -223,7 +233,10 @@
     raised = jnp.exp(logits - jnp.max(logits, axis=0, keepdims=True))
     rw = raised / jnp.sum(raised, axis=0, keepdims=True)
     ids = routes_in[...]
-    expert_of = lax.broadcasted_iota(jnp.int32, (EP, TP * PAD), 0)
+    place = lax.broadcasted_iota(jnp.int32, (EP, TP * PAD), 0)
+    expert_of = jnp.zeros((EP, TP * PAD), jnp.int32)
+    for p, d in enumerate(order):
+        expert_of = jnp.where(place == p, ep_shift(me, d, 1), expert_of)
     member = jnp.zeros((EP, TP * PAD), f32)
     weight = jnp.zeros((EP, TP * PAD), f32)
     for k in range(4):
@@ -280,6 +293,9 @@
     key_raw = mm_nt(normed, wkr[...]).astype(bf16)
     new_rope = rotate(key_raw.astype(f32)).astype(bf16)
     rope_ref[...] = new_rope
+    with jax.named_scope("turn0"):
+        for s in range(4):
+            turn(s)
     with jax.named_scope("wait_wq"):
         c_wq.wait()
         c_wqr.wait()
@@ -303,6 +319,9 @@
     for c in ph1:
         c.start()
     msg_r[t] = msg_s[t]
+    with jax.named_scope("turn1"):
+        for s in range(4, SEQ):
+            turn(s)
     with jax.named_scope("wait_tp1"):
         for c in ph1:
             c.wait()
@@ -342,60 +361,55 @@
         )
         ps_ref[s] = jnp.broadcast_to(total * scale, (16, 128))
     c_rope.wait()
-
-    def score(s, carry):
-        cache_copy(s).wait()
-        val = mm_nt(Q[s], cache[s]) + mm(Qr[s, :, 0:ROT], rope[s])
-        valid = lax.broadcasted_iota(jnp.int32, (16, LEN), 1) < lens[s]
-        S[s] = jnp.where(valid, val * scale, -jnp.inf)
-        return carry
-
-    with jax.named_scope("scores"):
-        lax.fori_loop(0, SEQ, score, 0, unroll=2)
-
-    def soft(s, carry):
-        sc = S[s]
-        own = ps_ref[s][:, 0:1]
-        highest = jnp.maximum(jnp.max(sc, axis=-1, keepdims=True), own)
-        e = jnp.exp(sc - highest)
-        eo = jnp.exp(own - highest)
-        total = jnp.sum(e, axis=-1, keepdims=True) + eo
-        Pb[s] = (e / total).astype(bf16)
-        ps_ref[s] = jnp.broadcast_to((eo / total).astype(bf16).astype(f32), (16, 128))
-        return carry
-
     for c in (c_wo, c_wg, c_wu, c_wd):
         c.start()
-    with jax.named_scope("softmax"):
-        lax.fori_loop(0, SEQ, soft, 0, unroll=4)
-
-    for s in range(SEQ):
-        val = mm(Pb[s], cache[s]) + ps_ref[s][:, 0:1] * nl32[s : s + 1, :]
-        for c in range(LAT // 128):
-            O.at[c][pl.ds(s, 16, stride=PAD), :] = val[:, c * 128 : (c + 1) * 128]
-    for j in range(TP):
-        for h in range(HL):
-            at = (j * HL + h) * PAD
+    for g in range(3):
+        group = range(4 * g, 4 * g + 4)
+        with jax.named_scope(f"attend{g}"):
+            for s in group:
+                val = mm(Q[s], turned[s]) + mm(Qr[s, :, 0:ROT], rope[s])
+                valid = lax.broadcasted_iota(jnp.int32, (16, LEN), 1) < lens[s]
+                S[s] = jnp.where(valid, val * scale, -jnp.inf)
+            for s in group:
+                sc = S[s]
+                own = ps_ref[s][:, 0:1]
+                highest = jnp.maximum(jnp.max(sc, axis=-1, keepdims=True), own)
+                e = jnp.exp(sc - highest)
+                eo = jnp.exp(own - highest)
+                total = jnp.sum(e, axis=-1, keepdims=True) + eo
+                Pb[s] = (e / total).astype(bf16)
+                ps_ref[s] = jnp.broadcast_to((eo / total).astype(bf16).astype(f32), (16, 128))
+            for s in group:
+                val = mm(Pb[s], cache[s]) + ps_ref[s][:, 0:1] * nl32[s : s + 1, :]
+                for c in range(LAT // 128):
+                    O.at[c][pl.ds(g * 64 + s % 4, 16, stride=4), :] = val[:, c * 128 : (c + 1) * 128]
             for c in range(LAT // 128):
-                hl_s[j, h, :, :, c * 128 : (c + 1) * 128] = (
-                    O[c, at : at + PAD, :].astype(bf16).reshape(3, 4, 128)
+                hl_s[g, :, :, :, c * 128 : (c + 1) * 128] = (
+                    O[c, g * 64 : (g + 1) * 64, :].astype(bf16).reshape(TP, HL, 4, 128)
                 )
-    ph2 = tp_copies(2, lambda j: hl_s.at[j], hl_r.at[t])
-    for c in ph2:
-        c.start()
-    hl_r[t] = hl_s[t]
+        for d in (2, 1, 3):
+            j = (t + d) % TP
+            pltpu.make_async_remote_copy(
+                src_ref=hl_s.at[g, j],
+                dst_ref=hl_r.at[g, t],
+                send_sem=hss,
+                recv_sem=hrs,
+                device_id={"tp": j},
+                device_id_type=MESH,
+            ).start()
+        hl_r[g, t] = hl_s[g, t]
     c_wo.wait()
     with jax.named_scope("wait_tp2"):
-        for c in ph2:
-            c.wait()
+        arrived(hl_r.at[:, 0:3], hrs)
+        arrived(hl_s.at[:, 0:3], hss)
     vals = jnp.concatenate(
-        [mm(hl_r[:, h].reshape(TP * PAD, LAT), wvh[h]).astype(bf16) for h in range(HL)], axis=1
+        [mm(hl_r[:, :, h].reshape(TP * PAD, LAT), wvh[h]).astype(bf16) for h in range(HL)], axis=1
     )
-    p_s[...] = mm(vals, wo[...]).astype(bf16).reshape(TP, 3, 4, D)
-    ph3 = tp_copies(3, lambda j: p_s.at[j], p_r.at[t])
+    p_s[...] = mm(vals, wo[...]).astype(bf16).reshape(3, TP, 4, D)
+    ph3 = tp_copies(3, lambda j: p_s.at[:, j], p_r.at[t])
     for c in ph3:
         c.start()
-    p_r[t] = p_s[t]
+    p_r[t] = p_s[:, t]
     with jax.named_scope("wait_tp3"):
         for c in ph3:
             c.wait()
@@ -415,23 +429,26 @@
         for c in ph4:
             c.wait()
 
-    X[...] = mm(Dm[...], gbuf[...].reshape(TP * PAD, D)).astype(bf16).reshape(EP, CAPP, D)
-    for p, d in enumerate(order):
-        if d:
-            e = ep_shift(me, d, 1)
-            pltpu.make_async_remote_copy(
-                src_ref=X.at[e],
-                dst_ref=R.at[p],
-                send_sem=dss,
-                recv_sem=drs.at[p // CHUNK],
-                device_id={"ep": e},
-                device_id_type=MESH,
-            ).start()
-        else:
-            R[p] = X[me]
-
-    def arrived(ref, sem):
-        pltpu.make_async_copy(ref, ref, sem).wait()
+    group_rows = gbuf[...].reshape(TP * PAD, D)
+    for k in range(4):
+        n = EP // 4
+        X[k * n : (k + 1) * n] = (
+            mm(Dm[k * n * CAPP : (k + 1) * n * CAPP, :], group_rows)
+            .astype(bf16)
+            .reshape(n, CAPP, D)
+        )
+        for p in range(k * n, (k + 1) * n):
+            if order[p]:
+                pltpu.make_async_remote_copy(
+                    src_ref=X.at[p],
+                    dst_ref=R.at[p],
+                    send_sem=dss,
+                    recv_sem=drs.at[p // CHUNK],
+                    device_id={"ep": ep_shift(me, order[p], 1)},
+                    device_id_type=MESH,
+                ).start()
+            else:
+                R[p] = X[p]
 
     for k in range(EP // CHUNK):
         lo, hi = k * CHUNK, (k + 1) * CHUNK
@@ -447,14 +464,14 @@
             if d:
                 pltpu.make_async_remote_copy(
                     src_ref=Y.at[p],
-                    dst_ref=T.at[me],
+                    dst_ref=T.at[p],
                     send_sem=ess,
                     recv_sem=ers,
                     device_id={"ep": ep_shift(me, d, -1)},
                     device_id_type=MESH,
                 ).start()
             else:
-                T[me] = Y[p]
+                T[p] = Y[p]
     with jax.named_scope("wait_return"):
         arrived(T.at[0 : EP - 1], ers)
     both = mm(Cm[...], T[...].reshape(EP * CAPP, D))
@@ -535,6 +552,7 @@
         V((TP, 3, 4, MSG), bf16),
         V((TP, 3, 4, MSG), bf16),
         V((SEQ, LEN, LAT), bf16),
+        V((SEQ, LAT, LEN), bf16),
         V((SEQ, ROT, LEN), bf16),
         V((LAT // 128, 16 * PAD, 128), f32),
         V((16 * PAD, 128), f32),
@@ -544,10 +562,10 @@
         V((SEQ, 16, LEN), bf16),
         V((SEQ, 16, 128), f32),
         V((LAT // 128, 16 * PAD, 128), f32),
-        V((TP, HL, 3, 4, LAT), bf16),
-        V((TP, HL, 3, 4, LAT), bf16),
+        V((3, TP, HL, 4, LAT), bf16),
+        V((3, TP, HL, 4, LAT), bf16),
         V((512, D), bf16),
-        V((TP, 3, 4, D), bf16),
+        V((3, TP, 4, D), bf16),
         V((TP, 3, 4, D), bf16),
         V((TP, 3, 4, D), bf16),
         V((PAD, D), f32),
@@ -567,6 +585,8 @@
         pltpu.SemaphoreType.DMA,
         pltpu.SemaphoreType.DMA((6, 4)),
         pltpu.SemaphoreType.DMA((6, 4)),
+        pltpu.SemaphoreType.DMA,
+        pltpu.SemaphoreType.DMA,
         pltpu.SemaphoreType.DMA,
         pltpu.SemaphoreType.DMA((EP // CHUNK,)),
         pltpu.SemaphoreType.DMA,

time: 73.3 us -> 69.6 us (0.950)
  Pallas kernels: 72.5 us -> 68.9 us
    pallas_call x1, Pallas kernels: 71.9 us -> 68.2 us  [body(): pl.pallas_call(layer_kernel, name='layer', out_shape=(pltpu.VMEM((SEQ, D)...]
where the time goes in v3:
time: 69.6 us; the launch traced here: 69.5 us
  Pallas kernels  68.9 us (99%)
    pallas_call x1, Pallas kernels, body(): pl.pallas_call(layer_kernel, name='layer', out_shape=(pltpu.VMEM((SEQ, D)...  68.2 us

profile of v3, /device:TPU:1, one launch (start us, length us, event | category | flops | bytes accessed | tf_op | source)
XLA Modules:
  0.0 69.5 jit_solution(5249937538414559663)
XLA Ops:
  0.6 68.2 %layer.1 = (bf16[12,2048]{1,0:T(8,128)(2,1)S(1)}, bf16[12,512]{1,0:T(8,128)(2,1)S(1)}, bf16[12,64]{1,0:T(8,128)(2,1)S(1)}) custom-call(s32[12]{0:T(128)} %h_lens.1, bf16[12,2048]{1,0:T(8,128)(2,1)} %h_tok.1, s32[4,48]{1,0:T(4,128)} %bitcast.8, f32[4,48]{1,0:T(4,128)} %bitcast.9, bf16[2048]{0:T(1024)(128)(2,1)} %h_attn.1, bf16[512]{0:T(512)(128)(2,1)} %h_lat.1, ...), custom_call_target="tpu_custom_call" | custom-call | tf_op jit(solution)/shard_map/layer/pallas_call | solution.py:595
  68.8 0.7 finish.1

commit v4 on v3

--- a/solution.py
+++ b/solution.py
@@ -36,8 +36,10 @@
 far_first = sorted(range(1, EP), key=lambda d: -(hops(d // 8) + hops((d // 2) % 4)))
 
 
-order = far_first + [0]
+order = far_first[::-1] + [0]
 CHUNK = 16
+QB = 128
+DA = D - TP * QB
 
 
 def ep_shift(me, d, sign):
@@ -124,7 +126,9 @@
     wo,
     p_s,
     p_r,
-    gbuf,
+    ffn_own,
+    g_quarter,
+    g_rest,
     mixed_ref,
     Dm,
     Cm,
@@ -144,10 +148,20 @@
     trs,
     hss,
     hrs,
+    YB,
+    SB,
     dss,
     drs,
     ess,
     ers,
+    dsb,
+    drb,
+    xgs,
+    xgr,
+    ybs,
+    ybr,
+    sbs,
+    sbr,
 ):
     me = lax.axis_index("ep")
     t = lax.axis_index("tp")
@@ -195,6 +209,10 @@
     def arrived(ref, sem):
         pltpu.make_async_copy(ref, ref, sem).wait()
 
+    def tp_wait(phase, src, dst):
+        arrived(dst, trs.at[phase])
+        arrived(src, tss.at[phase])
+
     def turn(s):
         cache_copy(s).wait()
         turned[s] = cache[s].T
@@ -207,8 +225,8 @@
                 pltpu.make_async_remote_copy(
                     src_ref=src(j),
                     dst_ref=dst,
-                    send_sem=tss.at[phase, d],
-                    recv_sem=trs.at[phase, d],
+                    send_sem=tss.at[phase],
+                    recv_sem=trs.at[phase],
                     device_id={"tp": j},
                     device_id_type=MESH,
                 )
@@ -301,30 +319,34 @@
         c_wqr.wait()
         c_wl.wait()
     with jax.named_scope("wait_tp0"):
-        for c in ph0:
-            c.wait()
+        tp_wait(0, nbuf.at[0:3], nbuf.at[0:3])
 
     rows = nbuf[...].reshape(TP * PAD, D)
     qp = mm(rows, wq[...]).astype(bf16)
-    for h in range(HL):
-        ql = mm_nt(qp[:, h * 128 : (h + 1) * 128], wkh[h]).astype(bf16)
-        msg_s[:, :, :, h * LAT : (h + 1) * LAT] = ql.reshape(TP, 3, 4, LAT)
-    msg_s[:, :, :, HL * LAT : HL * LAT + HL * ROT] = (
-        mm(rows, wqr[...]).astype(bf16).reshape(TP, 3, 4, HL * ROT)
-    )
-    msg_s[:, :, :, HL * LAT + HL * ROT :] = (
-        mm(rows, wl[...]).astype(bf16).reshape(TP, 3, 4, 128)
-    )
-    ph1 = tp_copies(1, lambda j: msg_s.at[j], msg_r.at[t])
-    for c in ph1:
-        c.start()
+    cut = 2 * LAT
+    for part in range(2):
+        for h in (2 * part, 2 * part + 1):
+            ql = mm_nt(qp[:, h * 128 : (h + 1) * 128], wkh[h]).astype(bf16)
+            msg_s[:, :, :, h * LAT : (h + 1) * LAT] = ql.reshape(TP, 3, 4, LAT)
+        if part:
+            msg_s[:, :, :, HL * LAT : HL * LAT + HL * ROT] = (
+                mm(rows, wqr[...]).astype(bf16).reshape(TP, 3, 4, HL * ROT)
+            )
+            msg_s[:, :, :, HL * LAT + HL * ROT :] = (
+                mm(rows, wl[...]).astype(bf16).reshape(TP, 3, 4, 128)
+            )
+        cols = pl.ds(cut, MSG - cut) if part else pl.ds(0, cut)
+        for c in tp_copies(
+            1 + part, lambda j: msg_s.at[j, :, :, cols], msg_r.at[t, :, :, cols]
+        ):
+            c.start()
     msg_r[t] = msg_s[t]
     with jax.named_scope("turn1"):
         for s in range(4, SEQ):
             turn(s)
     with jax.named_scope("wait_tp1"):
-        for c in ph1:
-            c.wait()
+        tp_wait(1, msg_s.at[0:3, :, :, 0:cut], msg_r.at[0:3, :, :, 0:cut])
+        tp_wait(2, msg_s.at[0:3, :, :, cut:], msg_r.at[0:3, :, :, cut:])
 
     lat_raw = jnp.concatenate([msg_r[j, :, :, MSG - 128 :].reshape(PAD, 128) for j in range(TP)], axis=1)
     new_latent = rms(lat_raw.astype(f32), g_lat[...].astype(f32)).astype(bf16)
@@ -377,7 +399,7 @@
                 e = jnp.exp(sc - highest)
                 eo = jnp.exp(own - highest)
                 total = jnp.sum(e, axis=-1, keepdims=True) + eo
-                Pb[s] = (e / total).astype(bf16)
+                Pb[s] = (e * (1.0 / total)).astype(bf16)
                 ps_ref[s] = jnp.broadcast_to((eo / total).astype(bf16).astype(f32), (16, 128))
             for s in group:
                 val = mm(Pb[s], cache[s]) + ps_ref[s][:, 0:1] * nl32[s : s + 1, :]
@@ -411,85 +433,139 @@
         c.start()
     p_r[t] = p_s[:, t]
     with jax.named_scope("wait_tp3"):
-        for c in ph3:
-            c.wait()
+        tp_wait(3, p_s.at[:, 0:3], p_r.at[0:3])
     attn = p_r[0].reshape(PAD, D).astype(f32)
     for j in range(1, TP):
         attn = attn + p_r[j].reshape(PAD, D).astype(f32)
     attn = attn.astype(bf16).astype(f32)
     mixed = (tok32[...] + rms(attn, g_post[...].astype(f32))).astype(bf16).astype(f32)
     mixed_ref[...] = mixed
-    gbuf[t] = rms(mixed, g_ffn[...].astype(f32)).astype(bf16).reshape(3, 4, D)
-    ph4 = tp_copies(4, lambda j: gbuf.at[t], gbuf.at[t])
-    for c in ph4:
+    ffn = rms(mixed, g_ffn[...].astype(f32)).astype(bf16)
+    ffn_own[...] = ffn.reshape(3, 4, D)
+    mine = pl.ds(pl.multiple_of(DA + QB * t, 128), QB)
+    rest = pl.ds(0, DA)
+    for c in tp_copies(
+        4, lambda j: ffn_own.at[:, :, pl.ds(pl.multiple_of(DA + QB * j, 128), QB)], g_quarter.at[t]
+    ):
         c.start()
+    for c in tp_copies(6, lambda j: ffn_own.at[:, :, rest], g_rest.at[t]):
+        c.start()
+    g_quarter[t] = ffn_own[:, :, mine]
+    g_rest[t] = ffn_own[:, :, rest]
     for c in (c_wg, c_wu, c_wd):
         c.wait()
     with jax.named_scope("wait_tp4"):
-        for c in ph4:
-            c.wait()
-
-    group_rows = gbuf[...].reshape(TP * PAD, D)
+        tp_wait(4, g_quarter.at[0:3], g_quarter.at[0:3])
+    def ep_send(src, dst, ssem, rsem, shift):
+        pltpu.make_async_remote_copy(
+            src_ref=src,
+            dst_ref=dst,
+            send_sem=ssem,
+            recv_sem=rsem,
+            device_id={"ep": shift},
+            device_id_type=MESH,
+        ).start()
+
+    X[:, :, mine] = (
+        mm(Dm[...], g_quarter[...].reshape(TP * PAD, QB)).astype(bf16).reshape(EP, CAPP, QB)
+    )
+    for p in range(EP - 1):
+        to = ep_shift(me, order[p], 1)
+        ep_send(X.at[p, :, mine], R.at[p, :, mine], dsb, drb.at[p // CHUNK], to)
+    R[EP - 1, :, mine] = X[EP - 1, :, mine]
+    with jax.named_scope("wait_tp6"):
+        tp_wait(6, g_rest.at[0:3], g_rest.at[0:3])
+    rows_rest = g_rest[...].reshape(TP * PAD, DA)
     for k in range(4):
         n = EP // 4
-        X[k * n : (k + 1) * n] = (
-            mm(Dm[k * n * CAPP : (k + 1) * n * CAPP, :], group_rows)
+        X[k * n : (k + 1) * n, :, rest] = (
+            mm(Dm[k * n * CAPP : (k + 1) * n * CAPP, :], rows_rest)
             .astype(bf16)
-            .reshape(n, CAPP, D)
+            .reshape(n, CAPP, DA)
         )
-        for p in range(k * n, (k + 1) * n):
-            if order[p]:
-                pltpu.make_async_remote_copy(
-                    src_ref=X.at[p],
-                    dst_ref=R.at[p],
-                    send_sem=dss,
-                    recv_sem=drs.at[p // CHUNK],
-                    device_id={"ep": ep_shift(me, order[p], 1)},
-                    device_id_type=MESH,
-                ).start()
-            else:
-                R[p] = X[p]
-
-    for k in range(EP // CHUNK):
-        lo, hi = k * CHUNK, (k + 1) * CHUNK
+        for p in range(k * n, min((k + 1) * n, EP - 1)):
+            to = ep_shift(me, order[p], 1)
+            ep_send(X.at[p, :, rest], R.at[p, :, rest], dss, drs.at[p // CHUNK], to)
+    R[EP - 1, :, rest] = X[EP - 1, :, rest]
+    chunks = [(k, k * CHUNK, (k + 1) * CHUNK, min((k + 1) * CHUNK, EP - 1)) for k in range(EP // CHUNK)]
+    for k, lo, hi, last in chunks:
+        with jax.named_scope(f"wait_quarter{k}"):
+            arrived(R.at[lo:last, :, mine], drb.at[k])
+        for d in (2, 1, 3):
+            pltpu.make_async_remote_copy(
+                src_ref=R.at[lo:hi, :, mine],
+                dst_ref=R.at[lo:hi, :, mine],
+                send_sem=xgs.at[k],
+                recv_sem=xgr.at[k],
+                device_id={"tp": (t + d) % TP},
+                device_id_type=MESH,
+            ).start()
+
+    for k, lo, hi, last in chunks:
         with jax.named_scope(f"wait_dispatch{k}"):
-            arrived(R.at[lo : min(hi, EP - 1)], drs.at[k])
+            arrived(R.at[lo:last, :, rest], drs.at[k])
+        with jax.named_scope(f"wait_gather{k}"):
+            arrived(R.at[lo:hi, :, 0 : 3 * QB], xgr.at[k])
         flat = R[lo:hi].reshape(CHUNK * CAPP, D)
         gate = jnp.minimum(mm(flat, wg[...]), clamp_limit)
         upward = jnp.clip(mm(flat, wu[...]), -clamp_limit, clamp_limit)
         active = ((upward + 1.0) * gate * jax.nn.sigmoid(sigmoid_alpha * gate)).astype(bf16)
         Y[lo:hi] = mm(active, wd[...]).astype(bf16).reshape(CHUNK, CAPP, D)
-        for p in range(lo, hi):
-            d = order[p]
-            if d:
-                pltpu.make_async_remote_copy(
-                    src_ref=Y.at[p],
-                    dst_ref=T.at[p],
-                    send_sem=ess,
-                    recv_sem=ers,
-                    device_id={"ep": ep_shift(me, d, -1)},
-                    device_id_type=MESH,
-                ).start()
-            else:
-                T[p] = Y[p]
+        for d in (2, 1, 3):
+            j = (t + d) % TP
+            pltpu.make_async_remote_copy(
+                src_ref=Y.at[lo:hi, :, pl.ds(pl.multiple_of(DA + QB * j, 128), QB)],
+                dst_ref=YB.at[t, lo:hi],
+                send_sem=ybs.at[k],
+                recv_sem=ybr.at[k],
+                device_id={"tp": j},
+                device_id_type=MESH,
+            ).start()
+        for p in range(lo, last):
+            to = ep_shift(me, order[p], -1)
+            ep_send(Y.at[p, :, rest], T.at[p, :, rest], ess, ers, to)
+        YB[t, lo:hi] = Y[lo:hi, :, mine]
+    T[EP - 1, :, rest] = Y[EP - 1, :, rest]
+    for k, lo, hi, last in chunks:
+        with jax.named_scope(f"wait_sum{k}"):
+            arrived(YB.at[0:3, lo:hi], ybr.at[k])
+        summed = YB[0, lo:hi].astype(f32)
+        for j in range(1, TP):
+            summed = summed + YB[j, lo:hi].astype(f32)
+        SB[lo:hi] = summed.astype(bf16)
+        for p in range(lo, last):
+            to = ep_shift(me, order[p], -1)
+            ep_send(SB.at[p], T.at[p, :, mine], sbs, sbr, to)
+    T[EP - 1, :, mine] = SB[EP - 1]
     with jax.named_scope("wait_return"):
-        arrived(T.at[0 : EP - 1], ers)
-    both = mm(Cm[...], T[...].reshape(EP * CAPP, D))
-    m_s[...] = (both[0 : TP * PAD] + both[TP * PAD :]).astype(bf16).reshape(TP, 3, 4, D)
+        arrived(T.at[0 : EP - 1, :, rest], ers)
+    with jax.named_scope("wait_return_sum"):
+        arrived(SB.at[0 : EP - 1], sbr)
+    for at, wide, cols in ((0, DA, rest), (DA, QB, mine)):
+        both = mm(Cm[...], T[:, :, cols].reshape(EP * CAPP, wide))
+        m_s[:, :, :, at : at + wide] = (
+            (both[0 : TP * PAD] + both[TP * PAD :]).astype(bf16).reshape(TP, 3, 4, wide)
+        )
     ph5 = tp_copies(5, lambda j: m_s.at[j], m_r.at[t])
     for c in ph5:
         c.start()
     m_r[t] = m_s[t]
     with jax.named_scope("wait_tp5"):
-        for c in ph5:
-            c.wait()
+        tp_wait(5, m_s.at[0:3], m_r.at[0:3])
+    arrived(X.at[0 : EP - 1, :, rest], dss)
+    arrived(X.at[0 : EP - 1, :, mine], dsb)
+    arrived(Y.at[0 : EP - 1, :, rest], ess)
+    arrived(SB.at[0 : EP - 1], sbs)
+    for k, lo, hi, last in chunks:
+        arrived(R.at[lo:hi, :, 0 : 3 * QB], xgs.at[k])
+        arrived(YB.at[0:3, lo:hi], ybs.at[k])
     with jax.named_scope("final"):
-      moe = m_r[0].reshape(PAD, D).astype(f32)
+      moe = m_r[0, :, :, 0:DA].reshape(PAD, DA).astype(f32)
       for j in range(1, TP):
-        moe = moe + m_r[j].reshape(PAD, D).astype(f32)
+        moe = moe + m_r[j, :, :, 0:DA].reshape(PAD, DA).astype(f32)
+      parts = [m_r[j, :, :, DA:].reshape(PAD, QB).astype(f32) for j in range(TP)]
+      moe = jnp.concatenate([moe] + parts, axis=1)
       moe = moe.astype(bf16).astype(f32)
-      arrived(X.at[0 : EP - 1], dss)
-      arrived(Y.at[0 : EP - 1], ess)
       res = (mixed_ref[...] + rms(moe, g_post2[...].astype(f32))).astype(bf16)
       out_ref[...] = res
 
@@ -567,7 +643,9 @@
         V((512, D), bf16),
         V((3, TP, 4, D), bf16),
         V((TP, 3, 4, D), bf16),
-        V((TP, 3, 4, D), bf16),
+        V((3, 4, D), bf16),
+        V((TP, 3, 4, QB), bf16),
+        V((TP, 3, 4, DA), bf16),
         V((PAD, D), f32),
         V((EP * CAPP, TP * PAD), bf16),
         V((2 * TP * PAD, EP * CAPP), bf16),
@@ -578,16 +656,26 @@
         V((D, 512), bf16),
         V((D, 512), bf16),
         V((512, D), bf16),
-        V((TP, 3, 4, D), bf16),
-        V((TP, 3, 4, D), bf16),
+        V((TP, 3, 4, DA + QB), bf16),
+        V((TP, 3, 4, DA + QB), bf16),
         pltpu.SemaphoreType.DMA((19,)),
         pltpu.SemaphoreType.DMA((SEQ,)),
         pltpu.SemaphoreType.DMA,
-        pltpu.SemaphoreType.DMA((6, 4)),
-        pltpu.SemaphoreType.DMA((6, 4)),
-        pltpu.SemaphoreType.DMA,
-        pltpu.SemaphoreType.DMA,
-        pltpu.SemaphoreType.DMA,
+        pltpu.SemaphoreType.DMA((7,)),
+        pltpu.SemaphoreType.DMA((7,)),
+        pltpu.SemaphoreType.DMA,
+        pltpu.SemaphoreType.DMA,
+        V((TP, EP, CAPP, QB), bf16),
+        V((EP, CAPP, QB), bf16),
+        pltpu.SemaphoreType.DMA,
+        pltpu.SemaphoreType.DMA((EP // CHUNK,)),
+        pltpu.SemaphoreType.DMA,
+        pltpu.SemaphoreType.DMA,
+        pltpu.SemaphoreType.DMA,
+        pltpu.SemaphoreType.DMA((EP // CHUNK,)),
+        pltpu.SemaphoreType.DMA((EP // CHUNK,)),
+        pltpu.SemaphoreType.DMA((EP // CHUNK,)),
+        pltpu.SemaphoreType.DMA((EP // CHUNK,)),
         pltpu.SemaphoreType.DMA((EP // CHUNK,)),
         pltpu.SemaphoreType.DMA,
         pltpu.SemaphoreType.DMA,

time: 69.6 us -> 64.5 us (0.927)
  Pallas kernels: 68.9 us -> 63.8 us
    pallas_call x1, Pallas kernels: 68.2 us -> 63.1 us  [body(): pl.pallas_call(layer_kernel, name='layer', out_shape=(pltpu.VMEM((SEQ, D)...]
where the time goes in v4:
time: 64.5 us; the launch traced here: 64.4 us
  Pallas kernels  63.8 us (99%)
  between operations  0.65 us (1%)
    pallas_call x1, Pallas kernels, body(): pl.pallas_call(layer_kernel, name='layer', out_shape=(pltpu.VMEM((SEQ, D)...  63.1 us

profile of v4, /device:TPU:1, one launch (start us, length us, event | category | flops | bytes accessed | tf_op | source)
XLA Modules:
  0.0 64.4 jit_solution(3381525318893658244)
XLA Ops:
  0.6 63.1 %layer.1 = (bf16[12,2048]{1,0:T(8,128)(2,1)S(1)}, bf16[12,512]{1,0:T(8,128)(2,1)S(1)}, bf16[12,64]{1,0:T(8,128)(2,1)S(1)}) custom-call(s32[12]{0:T(128)} %h_lens.1, bf16[12,2048]{1,0:T(8,128)(2,1)} %h_tok.1, s32[4,48]{1,0:T(4,128)} %bitcast.8, f32[4,48]{1,0:T(4,128)} %bitcast.9, bf16[2048]{0:T(1024)(128)(2,1)} %h_attn.1, bf16[512]{0:T(512)(128)(2,1)} %h_lat.1, ...), custom_call_target="tpu_custom_call" | custom-call | tf_op jit(solution)/shard_map/layer/pallas_call | solution.py:683
  63.8 0.7 %finish.1 = (bf16[12,2048]{1,0:T(8,128)(2,1)}, bf16[12,512]{1,0:T(8,128)(2,1)}, bf16[12,64]{1,0:T(8,128)(2,1)}) custom-call(bf16[12,2048]{1,0:T(8,128)(2,1)S(1)} %get-tuple-element.6.a, bf16[12,512]{1,0:T(8,128)(2,1)S(1)} %get-tuple-element.7.b, bf16[12,64]{1,0:T(8,128)(2,1)S(1)} %get-tuple-element.8.c), custom_call_target="tpu_custom_call" | custom-call | tf_op jit(solution)/shard_map/finish/pallas_call | solution.py:721

commit v5 on v4

--- a/solution.py
+++ b/solution.py
@@ -37,9 +37,11 @@
 
 
 order = far_first[::-1] + [0]
-CHUNK = 16
+CHUNK = 8
 QB = 128
 DA = D - TP * QB
+QR = 256
+DR = D - TP * QR
 
 
 def ep_shift(me, d, sign):
@@ -194,7 +196,7 @@
     c_ffn = local(h_ffn, g_ffn, 17)
     c_post2 = local(h_post2, g_post2, 18)
     small = (c_lens, c_routes, c_logits, c_lat, c_post, c_ffn, c_post2)
-    for c in (c_tok, c_attn) + small + (c_wku, c_wvu, c_wq, c_wqr, c_wl, c_wkr):
+    for c in (c_tok, c_attn) + small + (c_wku, c_wvu):
         c.start()
 
     def cache_copy(s):
@@ -202,9 +204,11 @@
 
     c_rope = pltpu.make_async_copy(h_crope, rope, rsem)
 
-    c_rope.start()
-    for s in range(SEQ):
-        cache_copy(s).start()
+    def fetch(g):
+        for s in range(4 * g, 4 * g + 4):
+            cache_copy(s).start()
+
+    fetch(0)
 
     def arrived(ref, sem):
         pltpu.make_async_copy(ref, ref, sem).wait()
@@ -241,7 +245,7 @@
     with jax.named_scope("wait_barrier"):
         pl.semaphore_wait(barrier, 34)
     ph0 = tp_copies(0, lambda j: nbuf.at[t], nbuf.at[t])
-    for c in ph0:
+    for c in ph0 + [c_wq, c_wqr, c_wl, c_wkr]:
         c.start()
 
     for c in small:
@@ -307,13 +311,11 @@
         wkh[h] = wtmp.at[0][pl.ds(h, LAT, stride=HL), :].astype(bf16)
         wvh[h] = wtmp.at[1][pl.ds(h, LAT, stride=HL), :].astype(bf16)
 
-    c_wkr.wait()
-    key_raw = mm_nt(normed, wkr[...]).astype(bf16)
-    new_rope = rotate(key_raw.astype(f32)).astype(bf16)
-    rope_ref[...] = new_rope
     with jax.named_scope("turn0"):
         for s in range(4):
             turn(s)
+    c_rope.start()
+    fetch(1)
     with jax.named_scope("wait_wq"):
         c_wq.wait()
         c_wqr.wait()
@@ -321,6 +323,7 @@
     with jax.named_scope("wait_tp0"):
         tp_wait(0, nbuf.at[0:3], nbuf.at[0:3])
 
+    fetch(2)
     rows = nbuf[...].reshape(TP * PAD, D)
     qp = mm(rows, wq[...]).astype(bf16)
     cut = 2 * LAT
@@ -341,6 +344,10 @@
         ):
             c.start()
     msg_r[t] = msg_s[t]
+    c_wkr.wait()
+    key_raw = mm_nt(normed, wkr[...]).astype(bf16)
+    new_rope = rotate(key_raw.astype(f32)).astype(bf16)
+    rope_ref[...] = new_rope
     with jax.named_scope("turn1"):
         for s in range(4, SEQ):
             turn(s)
@@ -444,6 +451,8 @@
     ffn_own[...] = ffn.reshape(3, 4, D)
     mine = pl.ds(pl.multiple_of(DA + QB * t, 128), QB)
     rest = pl.ds(0, DA)
+    mine_r = pl.ds(pl.multiple_of(DR + QR * t, 128), QR)
+    rest_r = pl.ds(0, DR)
     for c in tp_copies(
         4, lambda j: ffn_own.at[:, :, pl.ds(pl.multiple_of(DA + QB * j, 128), QB)], g_quarter.at[t]
     ):
@@ -514,7 +523,7 @@
         for d in (2, 1, 3):
             j = (t + d) % TP
             pltpu.make_async_remote_copy(
-                src_ref=Y.at[lo:hi, :, pl.ds(pl.multiple_of(DA + QB * j, 128), QB)],
+                src_ref=Y.at[lo:hi, :, pl.ds(pl.multiple_of(DR + QR * j, 128), QR)],
                 dst_ref=YB.at[t, lo:hi],
                 send_sem=ybs.at[k],
                 recv_sem=ybr.at[k],
@@ -523,9 +532,9 @@
             ).start()
         for p in range(lo, last):
             to = ep_shift(me, order[p], -1)
-            ep_send(Y.at[p, :, rest], T.at[p, :, rest], ess, ers, to)
-        YB[t, lo:hi] = Y[lo:hi, :, mine]
-    T[EP - 1, :, rest] = Y[EP - 1, :, rest]
+            ep_send(Y.at[p, :, rest_r], T.at[p, :, rest_r], ess, ers, to)
+        YB[t, lo:hi] = Y[lo:hi, :, mine_r]
+    T[EP - 1, :, rest_r] = Y[EP - 1, :, rest_r]
     for k, lo, hi, last in chunks:
         with jax.named_scope(f"wait_sum{k}"):
             arrived(YB.at[0:3, lo:hi], ybr.at[k])
@@ -535,13 +544,13 @@
         SB[lo:hi] = summed.astype(bf16)
         for p in range(lo, last):
             to = ep_shift(me, order[p], -1)
-            ep_send(SB.at[p], T.at[p, :, mine], sbs, sbr, to)
-    T[EP - 1, :, mine] = SB[EP - 1]
+            ep_send(SB.at[p], T.at[p, :, mine_r], sbs, sbr, to)
+    T[EP - 1, :, mine_r] = SB[EP - 1]
     with jax.named_scope("wait_return"):
-        arrived(T.at[0 : EP - 1, :, rest], ers)
+        arrived(T.at[0 : EP - 1, :, rest_r], ers)
     with jax.named_scope("wait_return_sum"):
         arrived(SB.at[0 : EP - 1], sbr)
-    for at, wide, cols in ((0, DA, rest), (DA, QB, mine)):
+    for at, wide, cols in ((0, DR, rest_r), (DR, QR, mine_r)):
         both = mm(Cm[...], T[:, :, cols].reshape(EP * CAPP, wide))
         m_s[:, :, :, at : at + wide] = (
             (both[0 : TP * PAD] + both[TP * PAD :]).astype(bf16).reshape(TP, 3, 4, wide)
@@ -554,16 +563,16 @@
         tp_wait(5, m_s.at[0:3], m_r.at[0:3])
     arrived(X.at[0 : EP - 1, :, rest], dss)
     arrived(X.at[0 : EP - 1, :, mine], dsb)
-    arrived(Y.at[0 : EP - 1, :, rest], ess)
+    arrived(Y.at[0 : EP - 1, :, rest_r], ess)
     arrived(SB.at[0 : EP - 1], sbs)
     for k, lo, hi, last in chunks:
         arrived(R.at[lo:hi, :, 0 : 3 * QB], xgs.at[k])
         arrived(YB.at[0:3, lo:hi], ybs.at[k])
     with jax.named_scope("final"):
-      moe = m_r[0, :, :, 0:DA].reshape(PAD, DA).astype(f32)
+      moe = m_r[0, :, :, 0:DR].reshape(PAD, DR).astype(f32)
       for j in range(1, TP):
-        moe = moe + m_r[j, :, :, 0:DA].reshape(PAD, DA).astype(f32)
-      parts = [m_r[j, :, :, DA:].reshape(PAD, QB).astype(f32) for j in range(TP)]
+        moe = moe + m_r[j, :, :, 0:DR].reshape(PAD, DR).astype(f32)
+      parts = [m_r[j, :, :, DR:].reshape(PAD, QR).astype(f32) for j in range(TP)]
       moe = jnp.concatenate([moe] + parts, axis=1)
       moe = moe.astype(bf16).astype(f32)
       res = (mixed_ref[...] + rms(moe, g_post2[...].astype(f32))).astype(bf16)
@@ -656,8 +665,8 @@
         V((D, 512), bf16),
         V((D, 512), bf16),
         V((512, D), bf16),
-        V((TP, 3, 4, DA + QB), bf16),
-        V((TP, 3, 4, DA + QB), bf16),
+        V((TP, 3, 4, DR + QR), bf16),
+        V((TP, 3, 4, DR + QR), bf16),
         pltpu.SemaphoreType.DMA((19,)),
         pltpu.SemaphoreType.DMA((SEQ,)),
         pltpu.SemaphoreType.DMA,
@@ -665,8 +674,8 @@
         pltpu.SemaphoreType.DMA((7,)),
         pltpu.SemaphoreType.DMA,
         pltpu.SemaphoreType.DMA,
-        V((TP, EP, CAPP, QB), bf16),
-        V((EP, CAPP, QB), bf16),
+        V((TP, EP, CAPP, QR), bf16),
+        V((EP, CAPP, QR), bf16),
         pltpu.SemaphoreType.DMA,
         pltpu.SemaphoreType.DMA((EP // CHUNK,)),
         pltpu.SemaphoreType.DMA,

time: 64.5 us -> 62.3 us (0.966)
  Pallas kernels: 63.8 us -> 61.3 us
    pallas_call x1, Pallas kernels: 63.1 us -> 60.6 us  [body(): pl.pallas_call(layer_kernel, name='layer', out_shape=(pltpu.VMEM((SEQ, D)...]
where the time goes in v5:
time: 62.3 us; the launch traced here: 62 us
  Pallas kernels  61.3 us (98%)
  between operations  0.65 us (1%)
    pallas_call x1, Pallas kernels, body(): pl.pallas_call(layer_kernel, name='layer', out_shape=(pltpu.VMEM((SEQ, D)...  60.6 us

profile of v5, /device:TPU:1, one launch (start us, length us, event | category | flops | bytes accessed | tf_op | source)
XLA Modules:
  0.0 62.0 jit_solution(18044211345113019387)
XLA Ops:
  0.6 60.6 %layer.1 = (bf16[12,2048]{1,0:T(8,128)(2,1)S(1)}, bf16[12,512]{1,0:T(8,128)(2,1)S(1)}, bf16[12,64]{1,0:T(8,128)(2,1)S(1)}) custom-call(s32[12]{0:T(128)} %h_lens.1, bf16[12,2048]{1,0:T(8,128)(2,1)} %h_tok.1, s32[4,48]{1,0:T(4,128)} %bitcast.8, f32[4,48]{1,0:T(4,128)} %bitcast.9, bf16[2048]{0:T(1024)(128)(2,1)} %h_attn.1, bf16[512]{0:T(512)(128)(2,1)} %h_lat.1, ...), custom_call_target="tpu_custom_call" | custom-call | tf_op jit(solution)/shard_map/layer/pallas_call | solution.py:692
  61.3 0.7 %finish.1 = (bf16[12,2048]{1,0:T(8,128)(2,1)}, bf16[12,512]{1,0:T(8,128)(2,1)}, bf16[12,64]{1,0:T(8,128)(2,1)}) custom-call(bf16[12,2048]{1,0:T(8,128)(2,1)S(1)} %get-tuple-element.6.a, bf16[12,512]{1,0:T(8,128)(2,1)S(1)} %get-tuple-element.7.b, bf16[12,64]{1,0:T(8,128)(2,1)S(1)} %get-tuple-element.8.c), custom_call_target="tpu_custom_call" | custom-call | tf_op jit(solution)/shard_map/finish/pallas_call | solution.py:730

commit v6 on v5

--- a/solution.py
+++ b/solution.py
@@ -38,6 +38,7 @@
 
 order = far_first[::-1] + [0]
 CHUNK = 8
+LAG = 3
 QB = 128
 DA = D - TP * QB
 QR = 256
@@ -510,6 +511,17 @@
                 device_id_type=MESH,
             ).start()
 
+    def sum_chunk(k, lo, hi, last):
+        with jax.named_scope(f"wait_sum{k}"):
+            arrived(YB.at[0:3, lo:hi], ybr.at[k])
+        summed = YB[0, lo:hi].astype(f32)
+        for j in range(1, TP):
+            summed = summed + YB[j, lo:hi].astype(f32)
+        SB[lo:hi] = summed.astype(bf16)
+        for p in range(lo, last):
+            to = ep_shift(me, order[p], -1)
+            ep_send(SB.at[p], T.at[p, :, mine_r], sbs, sbr, to)
+
     for k, lo, hi, last in chunks:
         with jax.named_scope(f"wait_dispatch{k}"):
             arrived(R.at[lo:last, :, rest], drs.at[k])
@@ -534,17 +546,11 @@
             to = ep_shift(me, order[p], -1)
             ep_send(Y.at[p, :, rest_r], T.at[p, :, rest_r], ess, ers, to)
         YB[t, lo:hi] = Y[lo:hi, :, mine_r]
+        if k >= LAG:
+            sum_chunk(*chunks[k - LAG])
     T[EP - 1, :, rest_r] = Y[EP - 1, :, rest_r]
-    for k, lo, hi, last in chunks:
-        with jax.named_scope(f"wait_sum{k}"):
-            arrived(YB.at[0:3, lo:hi], ybr.at[k])
-        summed = YB[0, lo:hi].astype(f32)
-        for j in range(1, TP):
-            summed = summed + YB[j, lo:hi].astype(f32)
-        SB[lo:hi] = summed.astype(bf16)
-        for p in range(lo, last):
-            to = ep_shift(me, order[p], -1)
-            ep_send(SB.at[p], T.at[p, :, mine_r], sbs, sbr, to)
+    for k in range(max(0, len(chunks) - LAG), len(chunks)):
+        sum_chunk(*chunks[k])
     T[EP - 1, :, mine_r] = SB[EP - 1]
     with jax.named_scope("wait_return"):
         arrived(T.at[0 : EP - 1, :, rest_r], ers)

time: 62.3 us -> 62.3 us (level)
  no operation moved by 1% of the time
where the time goes in v6:
time: 62.3 us; the launch traced here: 62 us
  Pallas kernels  61.3 us (98%)
  between operations  0.65 us (1%)
    pallas_call x1, Pallas kernels, body(): pl.pallas_call(layer_kernel, name='layer', out_shape=(pltpu.VMEM((SEQ, D)...  60.6 us

profile of v6, /device:TPU:1, one launch (start us, length us, event | category | flops | bytes accessed | tf_op | source)
XLA Modules:
  0.0 62.0 jit_solution(3316924519158846421)
XLA Ops:
  0.6 60.6 %layer.1 = (bf16[12,2048]{1,0:T(8,128)(2,1)S(1)}, bf16[12,512]{1,0:T(8,128)(2,1)S(1)}, bf16[12,64]{1,0:T(8,128)(2,1)S(1)}) custom-call(s32[12]{0:T(128)} %h_lens.1, bf16[12,2048]{1,0:T(8,128)(2,1)} %h_tok.1, s32[4,48]{1,0:T(4,128)} %bitcast.8, f32[4,48]{1,0:T(4,128)} %bitcast.9, bf16[2048]{0:T(1024)(128)(2,1)} %h_attn.1, bf16[512]{0:T(512)(128)(2,1)} %h_lat.1, ...), custom_call_target="tpu_custom_call" | custom-call | tf_op jit(solution)/shard_map/layer/pallas_call | solution.py:698
  61.3 0.7 %finish.1 = (bf16[12,2048]{1,0:T(8,128)(2,1)}, bf16[12,512]{1,0:T(8,128)(2,1)}, bf16[12,64]{1,0:T(8,128)(2,1)}) custom-call(bf16[12,2048]{1,0:T(8,128)(2,1)S(1)} %get-tuple-element.6.a, bf16[12,512]{1,0:T(8,128)(2,1)S(1)} %get-tuple-element.7.b, bf16[12,64]{1,0:T(8,128)(2,1)S(1)} %get-tuple-element.8.c), custom_call_target="tpu_custom_call" | custom-call | tf_op jit(solution)/shard_map/finish/pallas_call | solution.py:736
